TPU v7x, 256 devices: a 4x2x16 block of a 4x16x16 slice. The times are simulated.
256 devices in a mesh: grp: 2 (over y), sp: 16 (over z), tp: 8 (over x, core).
Axes of the slice: x: 4, y: 2, z: 16, core: 2. Of those that a mesh axis runs over, the one named last changes fastest.
The devices are a block of a 4x16x16 slice.
Arguments:
- layer_feed: bfloat16 [4, 8192, 4096], P('grp', 'sp'), parts along dimension 0, may hold values from -13 to 13
- address_mapping: bfloat16 [4096, 2048], P(None, 'tp'), may hold values from -0.09375 to 0.09375
- content_mapping: bfloat16 [4096, 2048], P(None, 'tp'), may hold values from -0.09375 to 0.09375
- beta_mapping_matrix: bfloat16 [4096, 32], replicated, may hold values from -0.032958984 to 0.029541016
- forgetting_mapping: bfloat16 [4096, 32], replicated, may hold values from -0.09375 to 0.09375
- logged_fading_speed: float32 [32], P('tp'), may hold values from -12 to -2.8
- extra_forgetting: bfloat16 [4, 8192, 32], P('grp', 'sp', 'tp'), parts along dimension 0, may hold values from -1.4 to 0
- opening_probe: bfloat16 [4, 2048], P('grp', 'tp'), parts along dimension 0, may hold values from -6 to 6
Outputs:
- context_memory_tensor: bfloat16 [4, 32, 64, 64], P('grp', 'tp', 'sp'), parts along dimension 0
- opening_normed_output: bfloat16 [4, 2048], P('grp', 'tp'), parts along dimension 0
There are 2 independent parts, one for each index of `grp`. A program takes and returns all parts, laid end to end along the dimension named above; an argument that names none is the same for every part. Nothing has to cross between parts.
All inputs are finite; a program needn't handle non-finite values.
Results may differ from a plain program's by a relative error of at most 0.014.
Values sent between devices are 32-bit elements; how exact they have to be, the bound alone decides.
A program may use at most 64 MiB of HBM per device.

v0:
```python
import math

import jax
import jax.numpy as jnp
from jax import lax
from jax.sharding import PartitionSpec as P

HEAD = 64


finest = lax.Precision.HIGHEST


def prefix(part, axis, combine, identity):
    count = lax.axis_size(axis)
    place = lax.axis_index(axis)
    ahead = count - 1 - place
    gathered = lax.all_gather(part, axis)
    state = jnp.zeros_like(part) + jnp.asarray(identity, part.dtype)

    def one(hop, state):
        source = count - 1 - hop
        return combine(state, lax.dynamic_index_in_dim(gathered, source, 0, False))

    return lax.fori_loop(0, ahead, one, state)


def in_blocks(x, dim, size):
    shape = x.shape
    pieces = x.reshape(*shape[:dim], size, shape[dim] // size, *shape[dim + 1 :])
    return jnp.moveaxis(pieces, dim, 0)


def sent_and_summed(x, axis, dim):
    pieces = in_blocks(x, dim, lax.axis_size(axis))
    arrived = lax.all_to_all(pieces, axis, split_axis=0, concat_axis=0, tiled=True)
    return arrived.sum(axis=0)


def sent_to_all(x, axis):
    size = lax.axis_size(axis)
    return lax.all_to_all(jnp.broadcast_to(x[None], (size, *x.shape)), axis, 0, 0, tiled=True)


def taken_together(x, axis):
    return sent_to_all(x, axis).sum(axis=0)


def head_columns(weight, heads):
    first = lax.axis_index("tp") * heads
    return lax.dynamic_slice_in_dim(weight, first, heads, 1)


def compute_states(
    address_embeddings,
    content_embeddings,
    beta_raw_scores,
    forgetting_raw_scores,
    extra_forgetting,
    logged_fading_speed,
):
    seqs, length, width = address_embeddings.shape
    heads = width // HEAD
    keys = jax.nn.silu(address_embeddings.astype(jnp.float32)).reshape(seqs, length, heads, HEAD)
    keys = keys * lax.rsqrt(jnp.sum(keys * keys, axis=-1, keepdims=True) + 1e-06)
    values = jax.nn.silu(content_embeddings.astype(jnp.float32)).reshape(seqs, length, heads, HEAD)
    betas = jax.nn.sigmoid(beta_raw_scores.astype(jnp.float32))
    decay_factors = -jnp.exp(logged_fading_speed) * jax.nn.softplus(
        forgetting_raw_scores.astype(jnp.float32)
    ) + extra_forgetting.astype(jnp.float32)
    groups = seqs * heads
    keys = keys.transpose(0, 2, 1, 3).reshape(groups, length, HEAD)
    values = values.transpose(0, 2, 1, 3).reshape(groups, length, HEAD)
    betas = betas.transpose(0, 2, 1).reshape(groups, length)
    decay_factors = decay_factors.transpose(0, 2, 1).reshape(groups, length)
    return (keys, values, betas, decay_factors)


def block_parts(keys, values, betas, decay_factors):
    groups, length, width = keys.shape
    size = math.gcd(length, 64)
    count = length // size
    keys = keys.reshape(groups, count, size, width)
    values = values.reshape(groups, count, size, width)
    betas = betas.reshape(groups, count, size)
    cumul = jnp.cumsum(decay_factors.reshape(groups, count, size), axis=-1)
    rows_idx = lax.broadcasted_iota(jnp.int32, (size, size), 0)
    cols_idx = lax.broadcasted_iota(jnp.int32, (size, size), 1)
    below = rows_idx > cols_idx
    spread = jnp.where(below, cumul[..., :, None] - cumul[..., None, :], 0.0)
    weights = jnp.where(below, jnp.exp(spread), 0.0)
    gram = jnp.einsum("gnid,gnjd->gnij", keys, keys, precision=finest)
    lower = jnp.eye(size, dtype=jnp.float32) + betas[..., :, None] * gram * weights
    right = jnp.concatenate(
        [values * betas[..., None], keys * (betas * jnp.exp(cumul))[..., None]], axis=-1
    )
    solved = jax.scipy.linalg.solve_triangular(lower, right, lower=True)
    update = solved[..., :width]
    mixing = solved[..., width:]
    carried = keys * jnp.exp(cumul[..., -1:] - cumul)[..., None]
    closing = jnp.exp(cumul[..., -1])
    return (update, mixing, carried, closing)


def run_blocks(start, parts, padding):

    def advance(state, piece):
        update, mixing, carried, closing = piece
        update = jnp.concatenate(
            [jnp.zeros(update.shape[:-1] + (padding,), jnp.float32), update], axis=-1
        )
        fresh = update - jnp.einsum("gck,gkw->gcw", mixing, state, precision=finest)
        state = closing[:, None, None] * state + jnp.einsum(
            "gck,gcw->gkw", carried, fresh, precision=finest
        )
        return (state, None)

    moved = tuple((jnp.moveaxis(member, 1, 0) for member in parts))
    final, _ = lax.scan(advance, start, moved)
    return final


def matmul(left, right):
    return jnp.einsum("shij,shjk->shik", left, right, precision=finest)


def body(
    layer_feed,
    address_mapping,
    content_mapping,
    beta_mapping_matrix,
    forgetting_mapping,
    logged_fading_speed,
    extra_forgetting,
    opening_probe,
):
    heads = address_mapping.shape[1] // HEAD
    seqs_all = layer_feed.shape[0]
    address_embeddings = jnp.dot(
        layer_feed, address_mapping, preferred_element_type=jnp.float32
    ).astype(jnp.bfloat16)
    content_embeddings = jnp.dot(
        layer_feed, content_mapping, preferred_element_type=jnp.float32
    ).astype(jnp.bfloat16)
    beta_raw_scores = jnp.dot(
        layer_feed, head_columns(beta_mapping_matrix, heads), preferred_element_type=jnp.float32
    ).astype(jnp.bfloat16)
    forgetting_raw_scores = jnp.dot(
        layer_feed, head_columns(forgetting_mapping, heads), preferred_element_type=jnp.float32
    ).astype(jnp.bfloat16)
    keys, values, betas, decay_factors = compute_states(
        address_embeddings,
        content_embeddings,
        beta_raw_scores,
        forgetting_raw_scores,
        extra_forgetting,
        logged_fading_speed,
    )
    parts = block_parts(keys, values, betas, decay_factors)
    opening = jnp.concatenate(
        [jnp.eye(HEAD, dtype=jnp.float32), jnp.zeros((HEAD, HEAD), jnp.float32)], axis=1
    )
    start = jnp.broadcast_to(opening, (seqs_all * heads, HEAD, 2 * HEAD))
    joined = run_blocks(start, parts, HEAD).reshape(seqs_all, heads, HEAD, 2 * HEAD)
    transfer = joined[..., :HEAD]
    offset = joined[..., HEAD:]
    identity = jnp.broadcast_to(jnp.eye(HEAD, dtype=jnp.float32), transfer.shape)
    rows = HEAD // lax.axis_size("sp")
    first_row = lax.axis_index("sp") * rows
    suffix = prefix(transfer, "sp", matmul, identity)
    terms = matmul(suffix, offset)
    final = sent_and_summed(terms, "sp", 2)
    context_memory_tensor = final.astype(jnp.bfloat16)
    query_per_head = opening_probe.reshape(seqs_all, heads, HEAD)
    query_rows = lax.dynamic_slice_in_dim(query_per_head, first_row, rows, 2).astype(jnp.float32)
    partial_read = jnp.einsum("shk,shkv->shv", query_rows, final, precision=finest)
    state_readout = taken_together(partial_read, "sp")
    state_readout = state_readout * lax.rsqrt(
        jnp.mean(state_readout * state_readout, axis=-1, keepdims=True) + 1e-06
    )
    opening_normed_output = state_readout.reshape(seqs_all, heads * HEAD).astype(jnp.bfloat16)
    return (context_memory_tensor, opening_normed_output)


def solution(mesh):
    in_specs = (
        P("grp", "sp", None),
        P(None, "tp"),
        P(None, "tp"),
        P(),
        P(),
        P("tp"),
        P("grp", "sp", "tp"),
        P("grp", "tp"),
    )
    out_specs = (P("grp", "tp", "sp", None), P("grp", "tp"))
    return jax.shard_map(body, mesh=mesh, in_specs=in_specs, out_specs=out_specs, check_vma=False)
```

profile of v0, /device:TPU:34, one launch (start us, length us, event | category | flops | bytes accessed | tf_op | source)
XLA Modules:
  0.0 567.1 jit_solution(1860633266186598040)
XLA Ops:
  7.3 0.8 exponential_negate_fusion
  8.1 5.7 %fusion.52 = f32[2,4,512]{2,1,0:T(4,128)S(1)} fusion(bf16[2,512,4]{1,2,0:T(4,128)(2,1)} %param.18, bf16[2,512,4096]{2,1,0:T(8,128)(2,1)} %param.12, bf16[4096,32]{0,1:T(8,128)(2,1)} %param.16, s32[]{:T(128)S(6)} %select_n.25, f32[4]{0:T(128)S(1)} %exponential_negate_fusion), kind=kOutput, calls=%fused_computation.71 | convolution fusion | flops 33599488 | bytes 8445972 | tf_op jit(solution)/shard_map/dot_general | solution.py:148
  13.9 1.9 reduce_window_sum.11
  15.9 5.7 %fusion.30 = f32[2,4,512]{2,1,0:T(4,128)S(1)} fusion(bf16[2,512,4096]{2,1,0:T(8,128)(2,1)} %param.12, bf16[4096,32]{0,1:T(8,128)(2,1)} %param.15, s32[]{:T(128)S(6)} %select_n.25), kind=kOutput, calls=%fused_computation.40 | convolution fusion | flops 33574912 | bytes 8437764 | tf_op jit(solution)/shard_map/dot_general | solution.py:145
  21.8 6.0 %multiply_reduce_fusion = (f32[2,512,4]{1,2,0:T(4,128)S(1)}, f32[2,512,256]{1,2,0:T(8,128)S(1)}) fusion(bf16[2,512,4096]{2,1,0:T(8,128)(2,1)} %param.12, bf16[4096,256]{1,0:T(8,128)(2,1)S(1)} %copy-done), kind=kOutput, calls=%fused_computation.53 | convolution fusion | flops 2149576704 | bytes 11550720 | tf_op jit(solution)/shard_map/dot_general | solution.py:139
  27.8 2.0 copy.67
  29.8 2.2 broadcast_multiply_fusion.2
  32.0 1.3 copy-done.3
  33.3 4.8 select_bitcast_fusion
  38.1 316.0 %custom-call.4 = f32[8,8,1,64,64]{3,4,2,1,0:T(8,128)} custom-call(f32[8,8,1,64,64]{4,3,2,1,0:T(8,128)} %select_bitcast_fusion), custom_call_target="InvertDiagBlocksLowerTriangular" | custom-call | tf_op jit(solution)/shard_map/jit(_solve_triangular)/vmap(vmap())/triangular_solve | solution.py:97
  354.1 6.5 %convert_multiply_fusion = f32[2,512,256]{1,2,0:T(8,128)S(1)} fusion(bf16[2,512,4096]{2,1,0:T(8,128)(2,1)} %param.12, bf16[4096,256]{1,0:T(8,128)(2,1)} %param.14), kind=kOutput, calls=%fused_computation.28 | convolution fusion | flops 2149056512 | bytes 11534336 | tf_op jit(solution)/shard_map/dot_general | solution.py:142
  360.6 1.9 copy.69
  362.5 2.3 broadcast_multiply_fusion.1
  364.9 2.3 broadcast_multiply_fusion
  367.2 4.1 fusion.10
  371.2 2.8 slice_bitcast_fusion
  374.1 31.9 %while.22 = (s32[]{:T(128)}, f32[8,64,128]{2,1,0:T(8,128)S(1)}, f32[8,8]{1,0:T(8,128)S(1)}, f32[8,8,64,64]{3,2,0,1:T(8,128)}, f32[8,8,64,64]{3,2,0,1:T(8,128)}, /*index=5*/f32[8,8,64,64]{3,2,0,1:T(8,128)}, s32[]{:T(128)}) while((s32[]{:T(128)}, f32[8,64,128]{2,1,0:T(8,128)S(1)}, f32[8,8]{1,0:T(8,128)S(1)}, f32[8,8,64,64]{3,2,0,1:T(8,128)}, ...), condition=%wide.region_3.4_spmd, body=%wide.region_2.3_spmd.sunk | while | flops 100859904 | bytes 2229429 | solution.py:119
  374.1 1.0 dynamic-slice_bitcast_fusion.3
  375.1 1.3 convolution_subtract_fusion.2
  376.5 1.6 convolution_add_fusion.2
  378.1 1.0 dynamic-slice_bitcast_fusion.3
  379.1 1.3 convolution_subtract_fusion.2
  380.4 1.6 convolution_add_fusion.2
  382.1 1.0 dynamic-slice_bitcast_fusion.3
  383.1 1.3 convolution_subtract_fusion.2
  384.4 1.6 convolution_add_fusion.2
  386.1 1.0 dynamic-slice_bitcast_fusion.3
  387.0 1.3 convolution_subtract_fusion.2
  388.4 1.6 convolution_add_fusion.2
  390.0 1.0 dynamic-slice_bitcast_fusion.3
  391.0 1.3 convolution_subtract_fusion.2
  392.4 1.6 convolution_add_fusion.2
  394.0 1.0 dynamic-slice_bitcast_fusion.3
  395.0 1.3 convolution_subtract_fusion.2
  396.4 1.6 convolution_add_fusion.2
  398.0 1.0 dynamic-slice_bitcast_fusion.3
  399.0 1.3 convolution_subtract_fusion.2
  400.4 1.6 convolution_add_fusion.2
  402.0 1.0 dynamic-slice_bitcast_fusion.3
  403.0 1.3 convolution_subtract_fusion.2
  404.3 1.6 convolution_add_fusion.2
  406.8 89.9 %all-gather.3.cloned.1.call-done = f32[32,4,64,64]{3,2,1,0:T(8,128)} async-done(((f32[2,4,64,64]{3,2,1,0:T(8,128)}), f32[32,4,64,64]{3,2,1,0:T(8,128)}) %all-gather.3.cloned.1.call-update) | async-done | bytes 2097168 | tf_op jit(solution)/shard_map/all_gather | solution.py:18
  496.8 24.2 %while.23 = (s32[]{:T(128)}, f32[2,4,64,64]{2,3,1,0:T(8,128)S(1)}, s32[]{:T(128)}, f32[16,2,4,64,64]{4,3,2,1,0:T(8,128)}, s32[]{:T(128)}, /*index=5*/s32[]{:T(128)}, s32[]{:T(128)}, s32[]{:T(128)}) while((s32[]{:T(128)}, f32[2,4,64,64]{2,3,1,0:T(8,128)S(1)}, s32[]{:T(128)}, f32[16,2,4,64,64]{4,3,2,1,0:T(8,128)}, s32[]{:T(128)}, ...), condition=%wide.region_5.6_spmd, body=%wide.region_4.5_spmd.sunk | while | flops 25165828 | bytes 786567 | solution.py:25
  496.8 1.6 convolution_bitcast_fusion.2
  498.4 1.6 convolution_bitcast_fusion.2
  500.1 1.6 convolution_bitcast_fusion.2
  501.7 1.6 convolution_bitcast_fusion.2
  503.3 1.6 convolution_bitcast_fusion.2
  504.9 1.6 convolution_bitcast_fusion.2
  506.5 1.6 convolution_bitcast_fusion.2
  508.1 1.6 convolution_bitcast_fusion.2
  509.7 1.6 convolution_bitcast_fusion.2
  511.3 1.6 convolution_bitcast_fusion.2
  512.9 1.6 convolution_bitcast_fusion.2
  514.6 1.6 convolution_bitcast_fusion.2
  516.2 1.6 convolution_bitcast_fusion.2
  517.8 1.6 convolution_bitcast_fusion.2
  519.4 1.6 convolution_bitcast_fusion.2
  521.7 0.9 reshape.84
  522.6 4.0 all-to-all-start
  526.7 12.5 %all-to-all-done = f32[16,1,2048]{2,1,0:T(1,128)S(1)} async-done(((f32[16,1,2048]{2,1,0:T(1,128)}), f32[16,1,2048]{2,1,0:T(1,128)S(1)}, u32[]{:S(2)}, u32[]{:S(2)}) %all-to-all-start) | async-done | bytes 131104 | tf_op jit(solution)/shard_map/all_to_all | solution.py:36
  539.7 0.9 reduce.2
  541.8 4.3 all-to-all-start.1
  546.7 11.8 %all-to-all-done.1 = f32[16,1,512]{2,1,0:T(1,128)S(1)} async-done(((f32[16,1,512]{2,1,0:T(1,128)}), f32[16,1,512]{2,1,0:T(1,128)S(1)}, u32[]{:S(2)}, u32[]{:S(2)}) %all-to-all-start.1) | async-done | bytes 32800 | tf_op jit(solution)/shard_map/all_to_all | solution.py:42
  (69 shorter events, 6.6 us)
Async XLA Ops:
  7.2 14.6 %copy-start = (bf16[4096,256]{1,0:T(8,128)(2,1)S(1)}, bf16[4096,256]{1,0:T(8,128)(2,1)}, u32[]{:S(2)}) copy-start(bf16[4096,256]{1,0:T(8,128)(2,1)} %param.13) | copy-start | bytes 6291460
  7.2 489.5 %all-gather.3.cloned.1.call-start = ((), (), s32[]{:S(2)}) async-start(), calls=%async_computation.2 | async-start | bytes 4456448 | tf_op jit(solution)/shard_map/all_gather | solution.py:18
  32.0 1.4 copy-start.3
  362.5 2.4 copy-start.4
  364.9 2.3 copy-start.5
  406.0 0.7 copy-start.1
  496.7 24.2 %copy-start.2 = (f32[8,64,128]{2,1,0:T(8,128)S(1)}, f32[8,64,128]{2,1,0:T(8,128)}, u32[]{:S(2)}) copy-start(f32[8,64,128]{2,1,0:T(8,128)} %copy-done.1) | copy-start | bytes 786436
  496.8 29.8 %copy-start.6 = (bf16[2,256]{1,0:T(2,128)(2,1)S(1)}, bf16[2,256]{1,0:T(2,128)(2,1)}, u32[]{:S(2)}) copy-start(bf16[2,256]{1,0:T(2,128)(2,1)} %param.19) | copy-start | bytes 3076
  522.6 16.6 %all-to-all-start = ((f32[16,1,2048]{2,1,0:T(1,128)}), f32[16,1,2048]{2,1,0:T(1,128)S(1)}, u32[]{:S(2)}, u32[]{:S(2)}) async-start(f32[16,1,2048]{2,1,0:T(1,128)} %reshape.84), calls=%async_computation | async-start | bytes 262144 | tf_op jit(solution)/shard_map/all_to_all | solution.py:36
  541.8 16.7 %all-to-all-start.1 = ((f32[16,1,512]{2,1,0:T(1,128)}), f32[16,1,512]{2,1,0:T(1,128)S(1)}, u32[]{:S(2)}, u32[]{:S(2)}) async-start(f32[16,1,512]{2,1,0:T(1,128)} %reshape.86), calls=%async_computation.1 | async-start | bytes 65536 | tf_op jit(solution)/shard_map/all_to_all | solution.py:42
Sparse Core Ops, SparseCore 0:
  406.8 89.8 all-gather.2
where the time goes:
time: 569 us; the launch traced here: 567 us
  other arithmetic  328 us (58%)
  waiting for transfers between devices  114 us (20%)
  matrix products  80.4 us (14%)
  local copies, waits for them, and re-layouts  20.7 us (4%)
  between operations  14.3 us (3%)
  starting transfers between devices  8.29 us (1%)
    another operation x1, other arithmetic, block_parts(): solved = jax.scipy.linalg.solve_triangular(lower, right, lower=True)  316 us
    all_gather x1, waiting for transfers between devices, prefix(): gathered = lax.all_gather(part, axis)  89.9 us
    dot_general x16, matrix products, matmul(): return jnp.einsum('shij,shjk->shik', left, right, precision=finest)  24 us
    dot_general x8, matrix products, advance(): jnp.einsum('gck,gcw->gkw', carried, fresh, precision=finest)  12.9 us
    all_to_all x1, waiting for transfers between devices, sent_and_summed(): lax.all_to_all(pieces, axis, split_axis=0, concat_axis=0, tiled=True)  12.5 us
    all_to_all x1, waiting for transfers between devices, sent_to_all(): lax.all_to_all(jnp.broadcast_to(x[None], (size, *x.shape)), axis, 0, 0, t...  11.8 us
  transfers between devices with their start and end apart: 3, of which 3 were waited for; matrix products, arithmetic and copies ran while one was open for 0% of the time, Pallas kernels for 0%

commit v1 on v0

v1 whole, which is shorter than its diff:
```python
import functools

import jax
import jax.numpy as jnp
from jax import lax
from jax.experimental import pallas as pl
from jax.experimental.pallas import tpu as pltpu
from jax.sharding import PartitionSpec as P

HEAD = 64
LANES = 128
CHUNK = 128
ROWS = 256
MESH = pl.DeviceIdType.MESH
F32 = jnp.float32
BF16 = jnp.bfloat16
NN = (((1,), (0,)), ((), ()))
NT = (((1,), (1,)), ((), ()))
TN = (((0,), (0,)), ((), ()))


def dot(left, right, dims=NN):
    return lax.dot_general(left, right, dims, preferred_element_type=F32)


def split(x):
    high = x.astype(BF16)
    return high, (x - high.astype(F32)).astype(BF16)


def matmul(left, right):
    lh, ll = split(left)
    rh, rl = split(right)
    wide = jnp.concatenate(
        [jnp.concatenate([rh, rl], axis=1), jnp.concatenate([rh, jnp.zeros_like(rh)], axis=1)], axis=0
    )
    both = dot(jnp.concatenate([lh, ll], axis=1), wide)
    return both[:, : right.shape[1]] + both[:, right.shape[1] :]


def iotas(shape):
    return lax.broadcasted_iota(jnp.int32, shape, 0), lax.broadcasted_iota(jnp.int32, shape, 1)


def swapped(x):
    return pltpu.roll(x, HEAD, 1)


def composed(later, earlier):
    i, j = iotas(later.shape)
    diagonal = (i < HEAD) == (j < HEAD)
    transfer = jnp.where(diagonal, swapped(later), 0.0)
    return matmul(transfer, earlier) + jnp.where(diagonal, later, 0.0)


def silu(x):
    return x / (1.0 + jnp.exp(-x))


def project(step, heads, all_heads, x_ref, w_ref, wg_ref, extra_ref, speed_ref, keys_ref, values_ref, cols_ref, turned_ref):
    rows = pl.ds(pl.multiple_of(step * ROWS, ROWS), ROWS)
    x = x_ref[rows, :]
    width = heads * HEAD
    both = dot(x, w_ref[...]).astype(BF16).astype(F32)
    gates = dot(x, wg_ref[...]).astype(BF16)
    keys = silu(both[:, :width])
    high, low = split(keys * keys)
    i, j = iotas((width, width))
    same = jnp.where(i // HEAD == j // HEAD, 1.0, 0.0).astype(BF16)
    squares = dot(high, same) + dot(low, same)
    keys_ref[rows, :] = keys * lax.rsqrt(squares + 1e-06)
    values_ref[rows, :] = silu(both[:, width:])

    first = lax.axis_index("tp") * heads
    i, j = iotas((LANES, LANES))
    taken = ((j < heads) & (i == first + j)) | (
        (j >= heads) & (j < 2 * heads) & (i == all_heads + first + j - heads)
    )
    pre = dot(gates, jnp.where(taken, 1.0, 0.0).astype(BF16))
    i, j = iotas((heads, LANES))
    extra = dot(extra_ref[rows, :], jnp.where(j == i + heads, 1.0, 0.0).astype(BF16))
    _, lane = iotas((1, LANES))
    speed = jnp.zeros((1, LANES), F32)
    for h in range(heads):
        speed = jnp.where(lane == heads + h, speed_ref[h], speed)
    beta = 1.0 / (1.0 + jnp.exp(-pre))
    plus = jnp.maximum(pre, 0.0) + jnp.log(1.0 + jnp.exp(-jnp.abs(pre)))
    decay = -jnp.exp(speed) * plus + extra
    i, j = iotas((CHUNK, CHUNK))
    until = jnp.where(i >= j, 1.0, 0.0)
    for part in range(ROWS // CHUNK):
        at = slice(part * CHUNK, (part + 1) * CHUNK)
        total = lax.dot_general(until, decay[at], NN, precision=lax.Precision.HIGHEST, preferred_element_type=F32)
        _, lane = iotas((CHUNK, LANES))
        mixed = jnp.where(lane < heads, beta[at], total)
        place = step * (ROWS // CHUNK) + part
        cols_ref[place] = mixed
        turned_ref[place] = jnp.transpose(mixed)[: 2 * heads]


def chunk_maps(place, heads, keys_ref, values_ref, cols_ref, turned_ref, maps_ref):
    rows = pl.ds(pl.multiple_of(place * CHUNK, CHUNK), CHUNK)
    cols = cols_ref[place]
    i, j = iotas((CHUNK, CHUNK))
    left = j < HEAD
    apart = jnp.where(i > j, i ^ j, 0)
    one = jnp.where(i == j, 1.0, 0.0)
    zero = jnp.zeros((CHUNK, LANES), BF16)
    heads_of = []
    for h in range(heads):
        pair = slice(h // 2 * LANES, (h // 2 + 1) * LANES)
        keys = keys_ref[rows, pair]
        mine = left if h % 2 == 0 else ~left
        kh, kl = split(keys)
        mh, ml = split(jnp.where(mine, keys, 0.0))
        wide = jnp.concatenate([jnp.concatenate([kh, kh], axis=1), jnp.concatenate([kl, zero], axis=1)], axis=0)
        both = dot(jnp.concatenate([mh, ml], axis=1), wide, NT)
        gram = both[:, :CHUNK] + both[:, CHUNK:]
        beta = jnp.broadcast_to(cols[:, h : h + 1], (CHUNK, LANES))
        total = jnp.broadcast_to(cols[:, heads + h : heads + h + 1], (CHUNK, LANES))
        ahead = jnp.broadcast_to(turned_ref[place, heads + h : heads + h + 1, :], (CHUNK, LANES))
        lower = jnp.where(i > j, beta * gram * jnp.exp(total - ahead), 0.0)
        heads_of.append((lower, beta, total))
    inverses = [one - jnp.where(apart == 1, lower, 0.0) for lower, _, _ in heads_of]
    level = 1
    while 2 << level <= CHUNK:
        here = (apart >> level) == 1
        inner = [matmul(jnp.where(here, low[0], 0.0), inv) for low, inv in zip(heads_of, inverses)]
        inverses = [inv - matmul(inv, inn) for inv, inn in zip(inverses, inner)]
        level += 1
    for p in range(heads // 2):
        pair = slice(p * LANES, (p + 1) * LANES)
        keys = keys_ref[rows, pair]
        values = values_ref[rows, pair]
        turned = swapped(keys)
        carried, solved, closing = [], [], []
        for h in (2 * p, 2 * p + 1):
            mine = left if h % 2 == 0 else ~left
            _, beta, total = heads_of[h]
            right = beta * jnp.where(mine, values, -jnp.exp(total) * turned)
            solved.append(matmul(inverses[h], right))
            last = total[CHUNK - 1 :, :]
            carried.append(jnp.where(mine, keys * jnp.exp(last - total), 0.0))
            closing.append(jnp.exp(last))
        ch, cl = split(jnp.concatenate(carried, axis=0))
        sh, sl = split(jnp.concatenate(solved, axis=0))
        both = dot(ch, jnp.concatenate([sh, sl], axis=1), TN)
        tile = both[:, :LANES] + both[:, LANES:] + dot(cl, sh, TN)
        kept = jnp.where(i < HEAD, jnp.broadcast_to(closing[0], tile.shape), jnp.broadcast_to(closing[1], tile.shape))
        maps_ref[place, p] = tile + jnp.where(j == (i ^ HEAD), kept, 0.0)


def remote(src, dst, send, recv, to):
    return pltpu.make_async_remote_copy(
        src_ref=src, dst_ref=dst, send_sem=send, recv_sem=recv, device_id={"sp": to}, device_id_type=MESH
    )


def exchange(ring, near, tiles, near_ref, head_ref, far_ref, rows_ref, final_ref, probe_ref, sems):
    send1, recv1, send2, recv2, send3, recv3 = sems
    far = ring // near
    me = lax.axis_index("sp")
    place, block = lax.rem(me, near), lax.div(me, near)

    copies = []
    for k in range(1, near):
        to = lax.rem(place + k, near)
        copies.append(
            remote(tiles.at[to], near_ref.at[place], send1.at[k], recv1.at[k], block * near + to)
        )
        copies[-1].start()
    near_ref[place] = tiles[place]
    for copy in copies:
        copy.wait_recv()
    tile = near_ref[0]
    for k in range(1, near):
        tile = composed(near_ref[k], tile)

    head_ref[0] = tile[:HEAD]
    head_ref[1] = swapped(tile[HEAD:])
    side = lax.rem(block, 2)
    for k in range(1, far):
        to = lax.rem(block + k, far)
        copies.append(
            remote(head_ref.at[lax.rem(to, 2)], far_ref.at[block], send2.at[k], recv2.at[k], to * near + place)
        )
        copies[-1].start()
    far_ref[block] = head_ref[side]
    for copy in copies[near - 1 :]:
        copy.wait_recv()
    i, j = iotas((HEAD, LANES))
    below = jnp.zeros((HEAD, LANES), F32)
    state = far_ref[0]
    for k in range(1, far):
        later = far_ref[k]
        transfer = jnp.where(j < HEAD, swapped(later), 0.0)
        state = matmul(transfer, jnp.concatenate([state, below], axis=0)) + later

    slot = place * 2 + side
    probe = jnp.broadcast_to(probe_ref[pl.ds(slot, 1), :], (8, LANES))
    read = matmul(probe, jnp.concatenate([state, below], axis=0))
    rows = HEAD // ring
    for d in range(ring):
        rows_ref[d, :rows] = state[d * rows : (d + 1) * rows]
        rows_ref[d, rows : rows + 1] = read[:1]
    beside = lax.rem(block + 1 + (far - 2) * (1 - lax.div(place, near // 2)), far)
    targets = [block * near + lax.rem(place + k, near) for k in range(1, near)]
    targets += [beside * near + k for k in range(near)]
    last = []
    for k, to in enumerate(targets):
        last.append(remote(rows_ref.at[to], final_ref.at[slot], send3.at[k], recv3.at[slot], to))
        last[-1].start()
    final_ref[slot] = rows_ref[me]
    slots = 2 * near
    for k in range(1, slots):
        other = lax.rem(slot + k, slots)
        remote(rows_ref.at[0], final_ref.at[other], send3.at[0], recv3.at[other], me).wait_recv()
    for copy in copies + last:
        copy.wait_send()


def kernel(
    ring,
    heads,
    all_heads,
    x_hbm,
    wk_hbm,
    wv_hbm,
    wb_hbm,
    wf_hbm,
    speed_ref,
    extra_ref,
    probe_ref,
    states_ref,
    reads_ref,
    x_ref,
    w_ref,
    wb_ref,
    wf_ref,
    wg_ref,
    keys_ref,
    values_ref,
    cols_ref,
    turned_ref,
    maps_ref,
    tiles,
    near_ref,
    head_ref,
    far_ref,
    rows_ref,
    final_ref,
    q_ref,
    local_sems,
    x_sems,
    send1,
    recv1,
    send2,
    recv2,
    send3,
    recv3,
):
    me = lax.axis_index("sp")
    barrier = pltpu.get_barrier_semaphore()

    @pl.loop(1, ring)
    def _(k):
        pl.semaphore_signal(barrier, inc=1, device_id={"sp": lax.rem(me + k, ring)}, device_id_type=MESH)

    width = heads * HEAD
    seqs, span, _ = x_hbm.shape
    weights = [
        pltpu.make_async_copy(wb_hbm, wb_ref, local_sems.at[0]),
        pltpu.make_async_copy(wf_hbm, wf_ref, local_sems.at[1]),
        pltpu.make_async_copy(wk_hbm, w_ref.at[:, :width], local_sems.at[2]),
        pltpu.make_async_copy(wv_hbm, w_ref.at[:, width:], local_sems.at[3]),
    ]
    for copy in weights:
        copy.start()
    steps = seqs * span // ROWS
    for step in range(steps):
        s, first = divmod(step * ROWS, span)
        pltpu.make_async_copy(
            x_hbm.at[s, pl.ds(first, ROWS)], x_ref.at[pl.ds(step * ROWS, ROWS)], x_sems.at[step]
        ).start()

    for s in range(seqs):
        for h in range(heads):
            pair = probe_ref[s : s + 1, h // 2 * LANES : (h // 2 + 1) * LANES].astype(F32)
            pair = pair if h % 2 == 0 else swapped(pair)
            _, lane = iotas((1, LANES))
            q_ref[s * heads + h : s * heads + h + 1, :] = jnp.where(lane < HEAD, pair, 0.0)

    weights[0].wait()
    weights[1].wait()
    wg_ref[...] = jnp.concatenate(
        [wb_ref[...], wf_ref[...], jnp.zeros((wb_ref.shape[0], LANES - 2 * all_heads), BF16)], axis=1
    )
    weights[2].wait()
    weights[3].wait()

    @pl.loop(0, steps)
    def _(step):
        pltpu.make_async_copy(
            x_hbm.at[0, pl.ds(0, ROWS)], x_ref.at[pl.ds(step * ROWS, ROWS)], x_sems.at[step]
        ).wait()
        project(step, heads, all_heads, x_ref, w_ref, wg_ref, extra_ref, speed_ref, keys_ref, values_ref, cols_ref, turned_ref)

    chunks = span // CHUNK

    @pl.loop(0, seqs * chunks)
    def _(place):
        chunk_maps(place, heads, keys_ref, values_ref, cols_ref, turned_ref, maps_ref)

    for s in range(seqs):
        for p in range(heads // 2):
            parts = [maps_ref[s * chunks + n, p] for n in range(chunks)]
            while len(parts) > 1:
                parts = [composed(parts[n + 1], parts[n]) for n in range(0, len(parts), 2)]
            tiles[s * (heads // 2) + p] = parts[0]

    pl.semaphore_wait(barrier, ring - 1)
    near = seqs * heads // 2
    exchange(
        ring, near, tiles, near_ref, head_ref, far_ref, rows_ref, final_ref, q_ref,
        (send1, recv1, send2, recv2, send3, recv3),
    )

    rows = HEAD // ring
    _, lane = iotas((1, LANES))
    lines = []
    for s in range(seqs):
        line = []
        for h in range(heads):
            got = final_ref[s * heads + h]
            states_ref[s, h] = got[:rows, :HEAD].astype(BF16)
            read = jnp.where(lane < HEAD, got[rows : rows + 1], 0.0)
            read = read * lax.rsqrt(jnp.sum(read * read, axis=1, keepdims=True) / HEAD + 1e-06)
            line.append(read)
        pairs = [line[2 * p] + swapped(line[2 * p + 1]) for p in range(heads // 2)]
        lines.append(jnp.concatenate(pairs, axis=1))
    reads_ref[...] = jnp.concatenate(lines, axis=0).astype(BF16)


def body(
    ring,
    layer_feed,
    address_mapping,
    content_mapping,
    beta_mapping_matrix,
    forgetting_mapping,
    logged_fading_speed,
    extra_forgetting,
    opening_probe,
):
    seqs, span, depth = layer_feed.shape
    width = address_mapping.shape[1]
    heads = width // HEAD
    all_heads = beta_mapping_matrix.shape[1]
    tokens = seqs * span
    near = seqs * heads // 2
    places = tokens // CHUNK
    hbm = pl.BlockSpec(memory_space=pl.ANY)
    vmem = pl.BlockSpec(memory_space=pltpu.VMEM)
    dma = pltpu.SemaphoreType.DMA
    return pl.pallas_call(
        functools.partial(kernel, ring, heads, all_heads),
        out_shape=(
            jax.ShapeDtypeStruct((seqs, heads, HEAD // ring, HEAD), BF16),
            jax.ShapeDtypeStruct((seqs, width), BF16),
        ),
        in_specs=[hbm] * 5 + [pl.BlockSpec(memory_space=pltpu.SMEM), vmem, vmem],
        out_specs=(vmem, vmem),
        scratch_shapes=[
            pltpu.VMEM((tokens, depth), BF16),
            pltpu.VMEM((depth, 2 * width), BF16),
            pltpu.VMEM((depth, all_heads), BF16),
            pltpu.VMEM((depth, all_heads), BF16),
            pltpu.VMEM((depth, LANES), BF16),
            pltpu.VMEM((tokens, width), F32),
            pltpu.VMEM((tokens, width), F32),
            pltpu.VMEM((places, CHUNK, LANES), F32),
            pltpu.VMEM((places, 2 * heads, LANES), F32),
            pltpu.VMEM((places, heads // 2, LANES, LANES), F32),
            pltpu.VMEM((near, LANES, LANES), F32),
            pltpu.VMEM((near, LANES, LANES), F32),
            pltpu.VMEM((2, HEAD, LANES), F32),
            pltpu.VMEM((ring // near, HEAD, LANES), F32),
            pltpu.VMEM((ring, 8, LANES), F32),
            pltpu.VMEM((2 * near, 8, LANES), F32),
            pltpu.VMEM((seqs * heads, LANES), F32),
            dma((4,)),
            dma((tokens // ROWS,)),
            dma((near,)),
            dma((near,)),
            dma((ring // near,)),
            dma((ring // near,)),
            dma((2 * near - 1,)),
            dma((2 * near,)),
        ],
        compiler_params=pltpu.CompilerParams(
            collective_id=0, has_side_effects=True, vmem_limit_bytes=56 * 1024 * 1024
        ),
    )(
        layer_feed,
        address_mapping,
        content_mapping,
        beta_mapping_matrix,
        forgetting_mapping,
        logged_fading_speed,
        extra_forgetting.reshape(tokens, heads),
        opening_probe,
    )


def solution(mesh):
    in_specs = (
        P("grp", "sp", None),
        P(None, "tp"),
        P(None, "tp"),
        P(),
        P(),
        P("tp"),
        P("grp", "sp", "tp"),
        P("grp", "tp"),
    )
    out_specs = (P("grp", "tp", "sp", None), P("grp", "tp"))
    return jax.shard_map(
        functools.partial(body, mesh.shape["sp"]),
        mesh=mesh,
        in_specs=in_specs,
        out_specs=out_specs,
        check_vma=False,
    )
```

time: 569 us -> 96.1 us (0.17)
  other arithmetic: 328 us -> 0 us
  waiting for transfers between devices: 114 us -> 0 us
  Pallas kernels: 0 us -> 86.4 us
  matrix products: 80.4 us -> 0 us
  between operations: 14.3 us -> 0.64 us
  local copies, waits for them, and re-layouts: 20.7 us -> 8.76 us
  starting transfers between devices: 8.29 us -> 0 us
    another operation x2 -> x0, other arithmetic: 318 us -> none  [the longest x1 316 us: block_parts(): solved = jax.scipy.linalg.solve_triangular(lower, right, lower=True)]
    all_gather x1 -> x0, waiting for transfers between devices: 89.9 us -> none  [prefix(): gathered = lax.all_gather(part, axis)]
    pallas_call x0 -> x1, Pallas kernels: none -> 86.4 us  [body(): pl.pallas_call(functools.partial(kernel, ring, heads, all_heads), out_sha...]
    dot_general x38 -> x0, matrix products: 76.4 us -> none  [the longest x16 24 us: matmul(): return jnp.einsum('shij,shjk->shik', left, right, precision=finest)]
    all_to_all x2 -> x0, waiting for transfers between devices: 24.3 us -> none  [the longest x1 12.5 us: sent_and_summed(): lax.all_to_all(pieces, axis, split_axis=0, concat_axis=0, tiled=True)]
    all_to_all x2 -> x0, starting transfers between devices: 8.23 us -> none  [the longest x1 4.28 us: sent_to_all(): lax.all_to_all(jnp.broadcast_to(x[None], (size, *x.shape)), axis, 0, 0, t...]
    squeeze x8 -> x0, local copies, waits for them, and re-layouts: 7.81 us -> none  [run_blocks(): final, _ = lax.scan(advance, start, moved)]
    mul x4 -> x0, other arithmetic: 6.91 us -> none  [the longest x1 2.34 us: block_parts(): values * betas[..., None]]
  transfers between devices with their start and end apart: 3 -> 0, of which waited for: 3 -> 0; matrix products, arithmetic and copies ran while one was open for 0% -> 0% of each run, Pallas kernels for 0% -> 0%
where the time goes in v1:
time: 96.1 us; the launch traced here: 95.8 us
  Pallas kernels  86.4 us (90%)
  local copies, waits for them, and re-layouts  8.76 us (9%)
    pallas_call x1, Pallas kernels, body(): pl.pallas_call(functools.partial(kernel, ring, heads, all_heads), out_sha...  86.4 us
    unnamed x5, local copies, waits for them, and re-layouts  8.76 us

profile of v1, /device:TPU:34, one launch (start us, length us, event | category | flops | bytes accessed | tf_op | source)
XLA Modules:
  0.0 95.8 jit_solution(17186715314563217704)
XLA Ops:
  0.6 1.6 %copy.10 = bf16[2,512,4]{2,1,0:T(8,128)(2,1)} copy(bf16[2,512,4]{1,2,0:T(4,128)(2,1)} %param.14) | data formatting | bytes 16384 | tf_op args[6]
  2.2 2.3 %copy.11.wb_hbm = bf16[4096,32]{1,0:T(8,128)(2,1)} copy(bf16[4096,32]{0,1:T(8,128)(2,1)} %param.11) | data formatting | bytes 524288 | tf_op args[3]
  4.5 2.3 %copy.12.wf_hbm = bf16[4096,32]{1,0:T(8,128)(2,1)} copy(bf16[4096,32]{0,1:T(8,128)(2,1)} %param.12) | data formatting | bytes 524288 | tf_op args[4]
  6.8 86.4 %shard_map.95 = (bf16[2,4,4,64]{3,2,1,0:T(4,128)(2,1)}, bf16[2,256]{1,0:T(2,128)(2,1)}) custom-call(bf16[2,512,4096]{2,1,0:T(8,128)(2,1)} %x_hbm.1, bf16[4096,256]{1,0:T(8,128)(2,1)} %wk_hbm.1, bf16[4096,256]{1,0:T(8,128)(2,1)} %wv_hbm.1, bf16[4096,32]{1,0:T(8,128)(2,1)} %copy.11.wb_hbm, bf16[4096,32]{1,0:T(8,128)(2,1)} %copy.12.wf_hbm, f32[4]{0:T(128)} %speed_ref.1, ...), custom_call_target="tpu_custom_call" | custom-call | tf_op jit(solution)/shard_map/pallas_call | solution.py:365
  93.2 1.3 %copy.15 = bf16[2,4,4,64]{3,2,1,0:T(4,128)(2,1)} copy(bf16[2,4,4,64]{3,2,1,0:T(4,128)(2,1)} %get-tuple-element.4) | data formatting | bytes 8192
  94.5 1.2 %copy.16 = bf16[2,256]{1,0:T(2,128)(2,1)} copy(bf16[2,256]{1,0:T(2,128)(2,1)} %get-tuple-element.5) | data formatting | bytes 2048

commit v2 on v1

v2 whole, which is shorter than its diff:
```python
import functools

import jax
import jax.numpy as jnp
from jax import lax
from jax.experimental import pallas as pl
from jax.experimental.pallas import tpu as pltpu
from jax.sharding import PartitionSpec as P

HEAD = 64
LANES = 128
CHUNK = 128
ROWS = 256
MESH = pl.DeviceIdType.MESH
F32 = jnp.float32
BF16 = jnp.bfloat16
NN = (((1,), (0,)), ((), ()))
NT = (((1,), (1,)), ((), ()))
TN = (((0,), (0,)), ((), ()))


def dot(left, right, dims=NN):
    return lax.dot_general(left, right, dims, preferred_element_type=F32)


def split(x):
    high = x.astype(BF16)
    return high, (x - high.astype(F32)).astype(BF16)


def matmul(left, right):
    lh, ll = split(left)
    rh, rl = split(right)
    wide = jnp.concatenate(
        [jnp.concatenate([rh, rl], axis=1), jnp.concatenate([rh, jnp.zeros_like(rh)], axis=1)], axis=0
    )
    both = dot(jnp.concatenate([lh, ll], axis=1), wide)
    return both[:, : right.shape[1]] + both[:, right.shape[1] :]


def iotas(shape):
    return lax.broadcasted_iota(jnp.int32, shape, 0), lax.broadcasted_iota(jnp.int32, shape, 1)


def swapped(x):
    return pltpu.roll(x, HEAD, 1)


def diagonal():
    i, j = iotas((LANES, LANES))
    return (i < HEAD) == (j < HEAD)


def composed(later, earlier):
    own = diagonal()
    return matmul(jnp.where(own, swapped(later), 0.0), earlier) + jnp.where(own, later, 0.0)


def silu(x):
    return x / (1.0 + jnp.exp(-x))


def halves(x):
    return jnp.concatenate(split(x), axis=1)


def stacked(left, right):
    count = left.shape[0]
    both = dot(jnp.concatenate(split(left), axis=0), right)
    both = both[:count] + both[count:]
    return both[:, :LANES] + both[:, LANES:]


def project(step, heads, x_ref, w_ref, gate_ref, extra_ref, speed_ref, keys_ref, values_ref, cols_ref, turned_ref):
    rows = pl.ds(pl.multiple_of(step * ROWS, ROWS), ROWS)
    x = x_ref[rows, :]
    width = heads * HEAD
    both = dot(x, w_ref[...]).astype(BF16).astype(F32)
    pre = dot(gate_ref[...], x, NT).astype(BF16).astype(F32)
    keys = silu(both[:, :width])
    high, low = split(keys * keys)
    i, j = iotas((width, width))
    same = jnp.where(i // HEAD == j // HEAD, 1.0, 0.0).astype(BF16)
    squares = dot(high, same) + dot(low, same)
    keys_ref[rows, :] = keys * lax.rsqrt(squares + 1e-06)
    values_ref[rows, :] = silu(both[:, width:])

    spans = extra_ref.shape[2] // ROWS
    at = pl.ds(pl.multiple_of(lax.rem(step, spans) * ROWS, ROWS), ROWS)
    extra = extra_ref[lax.div(step, spans), :, at].astype(F32)
    extra = jnp.concatenate([extra, jnp.zeros((8 - heads, ROWS), F32)], axis=0)
    i, _ = iotas((8, ROWS))
    speed = jnp.zeros((8, ROWS), F32)
    for h in range(heads):
        speed = jnp.where(i == h, speed_ref[h], speed)
    beta = 1.0 / (1.0 + jnp.exp(-pre[:8]))
    fade = pre[8:]
    plus = jnp.maximum(fade, 0.0) + jnp.log(1.0 + jnp.exp(-jnp.abs(fade)))
    decay = -jnp.exp(speed) * plus + extra
    i, j = iotas((CHUNK, CHUNK))
    until = jnp.where(i <= j, 1.0, 0.0)
    for part in range(ROWS // CHUNK):
        at = slice(part * CHUNK, (part + 1) * CHUNK)
        total = lax.dot_general(
            decay[:, at], until, NN, precision=lax.Precision.HIGHEST, preferred_element_type=F32
        )
        mixed = jnp.concatenate([beta[:, at], total], axis=0)
        place = step * (ROWS // CHUNK) + part
        turned_ref[place] = mixed
        cols_ref[place] = jnp.transpose(mixed)


def lower_part(place, h, keys_ref, cols_ref, turned_ref):
    rows = pl.ds(pl.multiple_of(place * CHUNK, CHUNK), CHUNK)
    i, j = iotas((CHUNK, CHUNK))
    keys = keys_ref[rows, h // 2 * LANES : (h // 2 + 1) * LANES]
    mine = (j < HEAD) if h % 2 == 0 else (j >= HEAD)
    kh, kl = split(keys)
    mh, ml = split(jnp.where(mine, keys, 0.0))
    wide = jnp.concatenate([jnp.concatenate([kh, kh], axis=1), jnp.concatenate([kl, jnp.zeros_like(kl)], axis=1)], axis=0)
    both = dot(jnp.concatenate([mh, ml], axis=1), wide, NT)
    gram = both[:, :CHUNK] + both[:, CHUNK:]
    beta = jnp.broadcast_to(cols_ref[place, :, h : h + 1], (CHUNK, LANES))
    total = jnp.broadcast_to(cols_ref[place, :, 8 + h : 9 + h], (CHUNK, LANES))
    ahead = jnp.broadcast_to(turned_ref[place, 8 + h : 9 + h, :], (CHUNK, LANES))
    return jnp.where(i > j, beta * gram * jnp.exp(total - ahead), 0.0)


def chunk_map(place, p, inverses, keys_ref, values_ref, cols_ref):
    rows = pl.ds(pl.multiple_of(place * CHUNK, CHUNK), CHUNK)
    pair = slice(p * LANES, (p + 1) * LANES)
    i, j = iotas((CHUNK, CHUNK))
    keys = keys_ref[rows, pair]
    values = values_ref[rows, pair]
    turned = swapped(keys)
    carried, solved, closing = [], [], []
    for h, inverse in zip((2 * p, 2 * p + 1), inverses):
        mine = (j < HEAD) if h % 2 == 0 else (j >= HEAD)
        beta = jnp.broadcast_to(cols_ref[place, :, h : h + 1], (CHUNK, LANES))
        total = jnp.broadcast_to(cols_ref[place, :, 8 + h : 9 + h], (CHUNK, LANES))
        solved.append(matmul(inverse, beta * jnp.where(mine, values, -jnp.exp(total) * turned)))
        last = total[CHUNK - 1 :, :]
        carried.append(jnp.where(mine, keys * jnp.exp(last - total), 0.0))
        closing.append(jnp.exp(last))
    ch, cl = split(jnp.concatenate(carried, axis=0))
    sh, sl = split(jnp.concatenate(solved, axis=0))
    both = dot(ch, jnp.concatenate([sh, sl], axis=1), TN)
    tile = both[:, :LANES] + both[:, LANES:] + dot(cl, sh, TN)
    kept = jnp.where(i < HEAD, jnp.broadcast_to(closing[0], tile.shape), jnp.broadcast_to(closing[1], tile.shape))
    return tile + jnp.where(j == (i ^ HEAD), kept, 0.0)


SMALL = 16


def sequence_maps(s, chunks, heads, keys_ref, values_ref, cols_ref, turned_ref, low_ref, near_low_ref, tiles):
    places = [s * chunks + n for n in range(chunks)]
    chains = [(n, h) for n in range(chunks) for h in range(heads)]
    count = CHUNK // SMALL
    i, j = iotas((CHUNK, CHUNK))
    same = (i // SMALL) == (j // SMALL)
    same_bf = jnp.where(same, 1.0, 0.0).astype(BF16)
    apart = jnp.where(i > j, i ^ j, 0)
    r, l = iotas((SMALL, LANES))
    c = l % SMALL
    close = jnp.where(r > c, r ^ c, 0)
    unit = jnp.where(r == c, 1.0, 0.0)

    state = []
    for slot, (n, h) in enumerate(chains):
        lower = lower_part(places[n], h, keys_ref, cols_ref, turned_ref)
        low_ref[slot] = halves(lower)
        inside = jnp.where(same, lower, 0.0)
        near_low_ref[slot] = halves(inside)
        packed = inside[:SMALL]
        for b in range(1, count):
            packed = packed + inside[b * SMALL : (b + 1) * SMALL]
        state.append(unit - jnp.where(close == 1, packed, 0.0))
    level = 1
    while 2 << level <= SMALL:
        inner = [stacked(x, near_low_ref[slot]) for slot, x in enumerate(state)]
        spread = []
        for x in state:
            high, low = split(x)
            high = jnp.concatenate([high] * count, axis=0) * same_bf
            low = jnp.concatenate([low] * count, axis=0) * same_bf
            spread.append(jnp.concatenate([high, low], axis=1))
        inner = [stacked(y, wide) for y, wide in zip(inner, spread)]
        state = [x - jnp.where((close >> level) == 1, y, 0.0) for x, y in zip(state, inner)]
        level += 1
    state = [jnp.where(same, jnp.concatenate([x] * count, axis=0), 0.0) for x in state]
    while 2 << level <= CHUNK:
        size = 1 << level
        odd = [slice(b * size, (b + 1) * size) for b in range(1, CHUNK // size, 2)]
        even = [slice(b * size, (b + 1) * size) for b in range(0, CHUNK // size, 2)]
        here = jnp.concatenate([apart[at] for at in odd], axis=0)
        part = [jnp.concatenate([x[at] for at in odd], axis=0) for x in state]
        inner = [stacked(x, low_ref[slot]) for slot, x in enumerate(part)]
        inner = [stacked(y, halves(x)) for y, x in zip(inner, state)]
        part = [x - jnp.where((here >> level) == 1, y, 0.0) for x, y in zip(part, inner)]
        state = [
            jnp.concatenate(
                [z for b, at in enumerate(even) for z in (x[at], y[b * size : (b + 1) * size])], axis=0
            )
            for x, y in zip(state, part)
        ]
        level += 1
    for p in range(heads // 2):
        parts = [
            chunk_map(places[n], p, state[n * heads + 2 * p : n * heads + 2 * p + 2], keys_ref, values_ref, cols_ref)
            for n in range(chunks)
        ]
        while len(parts) > 1:
            parts = [composed(parts[n + 1], parts[n]) for n in range(0, len(parts), 2)]
        tiles[s * (heads // 2) + p] = parts[0]


def remote(src, dst, send, recv, to):
    return pltpu.make_async_remote_copy(
        src_ref=src, dst_ref=dst, send_sem=send, recv_sem=recv, device_id={"sp": to}, device_id_type=MESH
    )


def greet(ring, near, me, barrier):
    far = ring // near
    place, block = lax.rem(me, near), lax.div(me, near)

    def tell(to):
        pl.semaphore_signal(barrier, inc=1, device_id={"sp": to}, device_id_type=MESH)

    for k in range(1, near):
        tell(block * near + lax.rem(place + k, near))

    @pl.when(block > 0)
    def _():
        tell(me - near)

    @pl.when(block < far - 1)
    def _():
        for k in range(near):
            tell((far - 1) * near + k)


def exchange(ring, near, me, tiles, near_ref, state_ref, prior_ref, rows_ref, final_ref, probe_ref, sems):
    recv1, send2, recv2, send3, recv3 = sems
    far = ring // near
    place, block = lax.rem(me, near), lax.div(me, near)
    own = diagonal()

    near_ref[place] = tiles[place]

    def arrived(k):
        @pl.when(place != k)
        def _():
            remote(tiles.at[0], near_ref.at[k], send2, recv1.at[k], me).wait_recv()

    arrived(0)
    tile = near_ref[0]
    for k in range(1, near - 1):
        arrived(k)
        tile = composed(near_ref[k], tile)

    carry = remote(state_ref, prior_ref, send2, recv2, lax.rem(me + near, ring))

    @pl.when(block == 0)
    def _():
        prior_ref[...] = jnp.zeros_like(prior_ref)

    @pl.when(block > 0)
    def _():
        carry.wait_recv()

    prior = prior_ref[...]
    state = composed(tile, jnp.where(own, jnp.concatenate([prior, prior], axis=0), 0.0))
    arrived(near - 1)
    state = composed(near_ref[near - 1], state)
    state = jnp.where(own, state, 0.0)
    both = state[:HEAD] + state[HEAD:]

    @pl.when(block < far - 1)
    def _():
        state_ref[...] = both
        carry.start()

    @pl.when(block == far - 1)
    def _():
        rows = HEAD // ring
        read = matmul(jnp.broadcast_to(probe_ref[pl.ds(place, 1), :], (8, LANES)), state)
        for d in range(ring):
            rows_ref[d, :rows] = both[d * rows : (d + 1) * rows]
            rows_ref[d, rows : rows + 1] = read[:1]

        @pl.loop(1, ring)
        def _(k):
            to = lax.rem(me + k, ring)
            remote(rows_ref.at[to], final_ref.at[place], send3.at[k], recv3.at[place], to).start()

        final_ref[place] = rows_ref[me]

    for k in range(near):
        @pl.when((block < far - 1) | (place != k))
        def _():
            remote(rows_ref.at[0], final_ref.at[k], send3.at[0], recv3.at[k], me).wait_recv()

    @pl.when(block < far - 1)
    def _():
        carry.wait_send()

    @pl.when(block == far - 1)
    def _():
        @pl.loop(1, ring)
        def _(k):
            remote(rows_ref.at[0], final_ref.at[place], send3.at[k], recv3.at[place], me).wait_send()


def kernel(
    ring,
    heads,
    all_heads,
    x_hbm,
    wk_hbm,
    wv_hbm,
    wb_hbm,
    wf_hbm,
    speed_ref,
    extra_ref,
    probe_ref,
    states_ref,
    reads_ref,
    x_ref,
    w_ref,
    wg_ref,
    gate_ref,
    keys_ref,
    values_ref,
    cols_ref,
    turned_ref,
    low_ref,
    near_low_ref,
    tiles,
    near_ref,
    state_ref,
    prior_ref,
    rows_ref,
    final_ref,
    q_ref,
    local_sems,
    x_sems,
    send1,
    recv1,
    send2,
    recv2,
    send3,
    recv3,
):
    me = lax.axis_index("sp")
    width = heads * HEAD
    seqs, span, _ = x_hbm.shape
    pairs = heads // 2
    near = seqs * pairs
    far = ring // near
    barrier = pltpu.get_barrier_semaphore()
    weights = [
        pltpu.make_async_copy(wb_hbm, wg_ref.at[:all_heads], local_sems.at[0]),
        pltpu.make_async_copy(wf_hbm, wg_ref.at[all_heads:], local_sems.at[1]),
        pltpu.make_async_copy(wk_hbm, w_ref.at[:, :width], local_sems.at[2]),
        pltpu.make_async_copy(wv_hbm, w_ref.at[:, width:], local_sems.at[3]),
    ]
    for copy in weights:
        copy.start()
    steps = span // ROWS
    for step in range(seqs * steps):
        s, first = divmod(step * ROWS, span)
        pltpu.make_async_copy(
            x_hbm.at[s, pl.ds(first, ROWS)], x_ref.at[pl.ds(step * ROWS, ROWS)], x_sems.at[step]
        ).start()
    greet(ring, near, me, barrier)
    for s in range(seqs):
        for p in range(pairs):
            q_ref[s * pairs + p : s * pairs + p + 1, :] = probe_ref[s : s + 1, p * LANES : (p + 1) * LANES].astype(F32)

    weights[0].wait()
    weights[1].wait()
    first = lax.axis_index("tp") * heads
    i, j = iotas((16, 2 * all_heads))
    taken = ((i < heads) & (j == first + i)) | ((i >= 8) & (i < 8 + heads) & (j == all_heads + first + i - 8))
    gate_ref[...] = dot(jnp.where(taken, 1.0, 0.0).astype(BF16), wg_ref[...]).astype(BF16)
    weights[2].wait()
    weights[3].wait()

    place, block = lax.rem(me, near), lax.div(me, near)

    def near_copy(pair):
        return remote(tiles.at[pair], near_ref.at[place], send1.at[pair], recv1.at[place], block * near + pair)

    @pl.loop(0, seqs)
    def _(s):
        @pl.loop(0, steps)
        def _(part):
            step = s * steps + part
            pltpu.make_async_copy(
                x_hbm.at[0, pl.ds(0, ROWS)], x_ref.at[pl.ds(step * ROWS, ROWS)], x_sems.at[step]
            ).wait()
            project(step, heads, x_ref, w_ref, gate_ref, extra_ref, speed_ref, keys_ref, values_ref, cols_ref, turned_ref)

        sequence_maps(
            s, span // CHUNK, heads, keys_ref, values_ref, cols_ref, turned_ref, low_ref, near_low_ref, tiles
        )

        @pl.when(s == 0)
        def _():
            pl.semaphore_wait(barrier, jnp.where(block == far - 1, ring - 1, near))

        for p in range(pairs):
            @pl.when(place != s * pairs + p)
            def _():
                near_copy(s * pairs + p).start()

    exchange(
        ring, near, me, tiles, near_ref, state_ref, prior_ref, rows_ref, final_ref, q_ref,
        (recv1, send2, recv2, send3, recv3),
    )
    for pair in range(near):
        @pl.when(place != pair)
        def _():
            near_copy(pair).wait_send()

    rows = HEAD // ring
    _, lane = iotas((1, LANES))
    for s in range(seqs):
        for p in range(pairs):
            got = final_ref[s * pairs + p]
            states_ref[s, 2 * p] = got[:rows, :HEAD].astype(BF16)
            states_ref[s, 2 * p + 1] = swapped(got)[:rows, :HEAD].astype(BF16)
            read = got[rows : rows + 1]
            square = read * read
            even = jnp.sum(jnp.where(lane < HEAD, square, 0.0), axis=1, keepdims=True)
            odd = jnp.sum(jnp.where(lane < HEAD, 0.0, square), axis=1, keepdims=True)
            mean = jnp.where(lane < HEAD, even, odd) / HEAD
            reads_ref[s : s + 1, p * LANES : (p + 1) * LANES] = (read * lax.rsqrt(mean + 1e-06)).astype(BF16)


def body(
    ring,
    layer_feed,
    address_mapping,
    content_mapping,
    beta_mapping_matrix,
    forgetting_mapping,
    logged_fading_speed,
    extra_forgetting,
    opening_probe,
):
    seqs, span, depth = layer_feed.shape
    width = address_mapping.shape[1]
    heads = width // HEAD
    all_heads = beta_mapping_matrix.shape[1]
    tokens = seqs * span
    near = seqs * heads // 2
    places = tokens // CHUNK
    chains = span // CHUNK * heads
    hbm = pl.BlockSpec(memory_space=pl.ANY)
    vmem = pl.BlockSpec(memory_space=pltpu.VMEM)
    dma = pltpu.SemaphoreType.DMA
    return pl.pallas_call(
        functools.partial(kernel, ring, heads, all_heads),
        out_shape=(
            jax.ShapeDtypeStruct((seqs, heads, HEAD // ring, HEAD), BF16),
            jax.ShapeDtypeStruct((seqs, width), BF16),
        ),
        in_specs=[hbm] * 5 + [pl.BlockSpec(memory_space=pltpu.SMEM), vmem, vmem],
        out_specs=(vmem, vmem),
        scratch_shapes=[
            pltpu.VMEM((tokens, depth), BF16),
            pltpu.VMEM((depth, 2 * width), BF16),
            pltpu.VMEM((2 * all_heads, depth), BF16),
            pltpu.VMEM((16, depth), BF16),
            pltpu.VMEM((tokens, width), F32),
            pltpu.VMEM((tokens, width), F32),
            pltpu.VMEM((places, CHUNK, 16), F32),
            pltpu.VMEM((places, 16, LANES), F32),
            pltpu.VMEM((chains, CHUNK, 2 * CHUNK), BF16),
            pltpu.VMEM((chains, CHUNK, 2 * CHUNK), BF16),
            pltpu.VMEM((near, LANES, LANES), F32),
            pltpu.VMEM((near, LANES, LANES), F32),
            pltpu.VMEM((HEAD, LANES), F32),
            pltpu.VMEM((HEAD, LANES), F32),
            pltpu.VMEM((ring, 8, LANES), F32),
            pltpu.VMEM((near, 8, LANES), F32),
            pltpu.VMEM((near, LANES), F32),
            dma((4,)),
            dma((tokens // ROWS,)),
            dma((near,)),
            dma((near,)),
            dma,
            dma,
            dma((ring,)),
            dma((near,)),
        ],
        compiler_params=pltpu.CompilerParams(
            collective_id=0, has_side_effects=True, vmem_limit_bytes=56 * 1024 * 1024
        ),
    )(
        layer_feed,
        address_mapping,
        content_mapping,
        beta_mapping_matrix.T,
        forgetting_mapping.T,
        logged_fading_speed,
        extra_forgetting.transpose(0, 2, 1),
        opening_probe,
    )


def solution(mesh):
    in_specs = (
        P("grp", "sp", None),
        P(None, "tp"),
        P(None, "tp"),
        P(),
        P(),
        P("tp"),
        P("grp", "sp", "tp"),
        P("grp", "tp"),
    )
    out_specs = (P("grp", "tp", "sp", None), P("grp", "tp"))
    return jax.shard_map(
        functools.partial(body, mesh.shape["sp"]),
        mesh=mesh,
        in_specs=in_specs,
        out_specs=out_specs,
        check_vma=False,
    )
```

time: 96.1 us -> 74.8 us (0.78)
  the two profiles are of different devices: /device:TPU:34 before, /device:TPU:160 now
where the time goes in v2:
time: 74.8 us; the launch traced here: 74.6 us
  Pallas kernels  71.5 us (96%)
  local copies, waits for them, and re-layouts  2.52 us (3%)
    pallas_call x1, Pallas kernels, body(): pl.pallas_call(functools.partial(kernel, ring, heads, all_heads), out_sha...  71.5 us
    unnamed x2, local copies, waits for them, and re-layouts  2.52 us

profile of v2, /device:TPU:160, one launch (start us, length us, event | category | flops | bytes accessed | tf_op | source)
XLA Modules:
  0.0 74.6 jit_solution(15911095782671284884)
XLA Ops:
  0.6 71.5 %shard_map.95 = (bf16[2,4,4,64]{3,2,1,0:T(4,128)(2,1)}, bf16[2,256]{1,0:T(2,128)(2,1)}) custom-call(bf16[2,512,4096]{2,1,0:T(8,128)(2,1)} %x_hbm.1, bf16[4096,256]{1,0:T(8,128)(2,1)} %wk_hbm.1, bf16[4096,256]{1,0:T(8,128)(2,1)} %wv_hbm.1, bf16[32,4096]{1,0:T(8,128)(2,1)} %bitcast.3, bf16[32,4096]{1,0:T(8,128)(2,1)} %bitcast.4, f32[4]{0:T(128)} %speed_ref.1, ...), custom_call_target="tpu_custom_call" | custom-call | tf_op jit(solution)/shard_map/pallas_call | solution.py:465
  72.1 1.3 %copy.12 = bf16[2,4,4,64]{3,2,1,0:T(4,128)(2,1)} copy(bf16[2,4,4,64]{3,2,1,0:T(4,128)(2,1)} %get-tuple-element.4) | data formatting | bytes 8192
  73.4 1.2 %copy.13 = bf16[2,256]{1,0:T(2,128)(2,1)} copy(bf16[2,256]{1,0:T(2,128)(2,1)} %get-tuple-element.5) | data formatting | bytes 2048

commit v3 on v2

v3 whole, which is shorter than its diff:
```python
import functools

import jax
import jax.numpy as jnp
from jax import lax
from jax.experimental import pallas as pl
from jax.experimental.pallas import tpu as pltpu
from jax.sharding import PartitionSpec as P

HEAD = 64
LANES = 128
CHUNK = 128
ROWS = 256
PIECES = 4
MESH = pl.DeviceIdType.MESH
F32 = jnp.float32
BF16 = jnp.bfloat16
NN = (((1,), (0,)), ((), ()))
NT = (((1,), (1,)), ((), ()))
TN = (((0,), (0,)), ((), ()))


def dot(left, right, dims=NN):
    return lax.dot_general(left, right, dims, preferred_element_type=F32)


def split(x):
    high = x.astype(BF16)
    return high, (x - high.astype(F32)).astype(BF16)


def matmul(left, right):
    lh, ll = split(left)
    rh, rl = split(right)
    wide = jnp.concatenate(
        [jnp.concatenate([rh, rl], axis=1), jnp.concatenate([rh, jnp.zeros_like(rh)], axis=1)], axis=0
    )
    both = dot(jnp.concatenate([lh, ll], axis=1), wide)
    return both[:, : right.shape[1]] + both[:, right.shape[1] :]


def iotas(shape):
    return lax.broadcasted_iota(jnp.int32, shape, 0), lax.broadcasted_iota(jnp.int32, shape, 1)


def swapped(x):
    return pltpu.roll(x, HEAD, 1)


def diagonal():
    i, j = iotas((LANES, LANES))
    return (i < HEAD) == (j < HEAD)


def composed(later, earlier):
    own = diagonal()
    return matmul(jnp.where(own, swapped(later), 0.0), earlier) + jnp.where(own, later, 0.0)


def silu(x):
    return x / (1.0 + jnp.exp(-x))


def project(
    step, heads, pieces, x_ref, w_ref, gate_ref, extra_ref, speed_ref, keys_ref, values_ref, cols_ref, turned_ref
):
    rows = pl.ds(pl.multiple_of(step * ROWS, ROWS), ROWS)
    width = heads * HEAD
    depth = x_ref.shape[1] // len(pieces)
    both = pre = None
    for k, arrive in enumerate(pieces):
        arrive()
        at = slice(k * depth, (k + 1) * depth)
        x = x_ref[rows, at]
        part, gates = dot(x, w_ref[at, :]), dot(gate_ref[:, at], x, NT)
        both, pre = (part, gates) if k == 0 else (both + part, pre + gates)
    both = both.astype(BF16).astype(F32)
    pre = pre.astype(BF16).astype(F32)
    keys = silu(both[:, :width])
    i, j = iotas((width, width))
    same = jnp.where(i // HEAD == j // HEAD, 1.0, 0.0).astype(BF16)
    squares = dot((keys * keys).astype(BF16), same)
    keys_ref[rows, :] = (keys * lax.rsqrt(squares + 1e-06)).astype(BF16)
    values_ref[rows, :] = silu(both[:, width:]).astype(BF16)

    spans = extra_ref.shape[2] // ROWS
    at = pl.ds(pl.multiple_of(lax.rem(step, spans) * ROWS, ROWS), ROWS)
    extra = extra_ref[lax.div(step, spans), :, at].astype(F32)
    extra = jnp.concatenate([extra, jnp.zeros((8 - heads, ROWS), F32)], axis=0)
    i, _ = iotas((8, ROWS))
    speed = jnp.zeros((8, ROWS), F32)
    for h in range(heads):
        speed = jnp.where(i == h, speed_ref[h], speed)
    beta = 1.0 / (1.0 + jnp.exp(-pre[:8]))
    fade = pre[8:]
    plus = jnp.maximum(fade, 0.0) + jnp.log(1.0 + jnp.exp(-jnp.abs(fade)))
    decay = -jnp.exp(speed) * plus + extra
    i, j = iotas((CHUNK, CHUNK))
    until = jnp.where(i <= j, 1.0, 0.0)
    for part in range(ROWS // CHUNK):
        at = slice(part * CHUNK, (part + 1) * CHUNK)
        total = lax.dot_general(
            decay[:, at], until, NN, precision=lax.Precision.HIGHEST, preferred_element_type=F32
        )
        mixed = jnp.concatenate([beta[:, at], total], axis=0)
        place = step * (ROWS // CHUNK) + part
        turned_ref[place] = mixed
        cols_ref[place] = jnp.transpose(mixed)


def lower_parts(place, p, keys_ref, cols_ref, turned_ref):
    rows = pl.ds(pl.multiple_of(place * CHUNK, CHUNK), CHUNK)
    i, j = iotas((CHUNK, CHUNK))
    left = jnp.where(j < HEAD, 1.0, 0.0).astype(BF16)
    keys = keys_ref[rows, p * LANES : (p + 1) * LANES]
    even = keys * left
    gram = dot(jnp.concatenate([even, keys - even], axis=0), keys, NT)
    parts = []
    for side in range(2):
        h = 2 * p + side
        beta = jnp.broadcast_to(cols_ref[place, :, h : h + 1], (CHUNK, LANES))
        total = jnp.broadcast_to(cols_ref[place, :, 8 + h : 9 + h], (CHUNK, LANES))
        ahead = jnp.broadcast_to(turned_ref[place, 8 + h : 9 + h, :], (CHUNK, LANES))
        lower = beta * gram[side * CHUNK : (side + 1) * CHUNK] * jnp.exp(total - ahead)
        parts.append(jnp.where(i > j, lower, 0.0).astype(BF16))
    return parts


def chunk_map(place, p, inverses, keys_ref, values_ref, cols_ref):
    rows = pl.ds(pl.multiple_of(place * CHUNK, CHUNK), CHUNK)
    pair = slice(p * LANES, (p + 1) * LANES)
    i, j = iotas((CHUNK, CHUNK))
    keys = keys_ref[rows, pair].astype(F32)
    values = values_ref[rows, pair].astype(F32)
    turned = swapped(keys)
    carried, solved, closing = [], [], []
    for h, inverse in zip((2 * p, 2 * p + 1), inverses):
        mine = (j < HEAD) if h % 2 == 0 else (j >= HEAD)
        beta = jnp.broadcast_to(cols_ref[place, :, h : h + 1], (CHUNK, LANES))
        total = jnp.broadcast_to(cols_ref[place, :, 8 + h : 9 + h], (CHUNK, LANES))
        right = beta * jnp.where(mine, values, -jnp.exp(total) * turned)
        solved.append(dot(inverse, right.astype(BF16)).astype(BF16))
        last = total[CHUNK - 1 :, :]
        carried.append(jnp.where(mine, keys * jnp.exp(last - total), 0.0).astype(BF16))
        closing.append(jnp.exp(last))
    tile = dot(jnp.concatenate(carried, axis=0), jnp.concatenate(solved, axis=0), TN)
    kept = jnp.where(i < HEAD, jnp.broadcast_to(closing[0], tile.shape), jnp.broadcast_to(closing[1], tile.shape))
    return tile + jnp.where(j == (i ^ HEAD), kept, 0.0)


SMALL = 16


def sequence_maps(s, chunks, heads, keys_ref, values_ref, cols_ref, turned_ref, low_ref, tiles):
    places = [s * chunks + n for n in range(chunks)]
    count = CHUNK // SMALL
    i, j = iotas((CHUNK, CHUNK))
    same = jnp.where((i // SMALL) == (j // SMALL), 1.0, 0.0).astype(BF16)
    apart = jnp.where(i > j, i ^ j, 0)
    r, l = iotas((SMALL, LANES))
    c = l % SMALL
    close = jnp.where(r > c, r ^ c, 0)
    unit = jnp.where(r == c, 1.0, 0.0)

    state = []
    for n in range(chunks):
        for p in range(heads // 2):
            for lower in lower_parts(places[n], p, keys_ref, cols_ref, turned_ref):
                low_ref[len(state)] = lower
                inside = lower * same
                packed = inside[:SMALL]
                for b in range(1, count):
                    packed = packed + inside[b * SMALL : (b + 1) * SMALL]
                state.append((unit - jnp.where(close == 1, packed.astype(F32), 0.0)).astype(BF16))
    level = 1
    while 2 << level <= SMALL:
        inner = [dot(x, low_ref[slot] * same).astype(BF16) for slot, x in enumerate(state)]
        inner = [dot(y, jnp.concatenate([x] * count, axis=0) * same) for x, y in zip(state, inner)]
        state = [x - jnp.where((close >> level) == 1, y, 0.0).astype(BF16) for x, y in zip(state, inner)]
        level += 1
    state = [jnp.concatenate([x] * count, axis=0) * same for x in state]
    while 2 << level <= CHUNK:
        size = 1 << level
        odd = [slice(b * size, (b + 1) * size) for b in range(1, CHUNK // size, 2)]
        even = [slice(b * size, (b + 1) * size) for b in range(0, CHUNK // size, 2)]
        here = jnp.concatenate([apart[at] for at in odd], axis=0)
        part = [jnp.concatenate([x[at] for at in odd], axis=0) for x in state]
        inner = [dot(x, low_ref[slot]).astype(BF16) for slot, x in enumerate(part)]
        inner = [dot(y, x) for y, x in zip(inner, state)]
        part = [x - jnp.where((here >> level) == 1, y, 0.0).astype(BF16) for x, y in zip(part, inner)]
        state = [
            jnp.concatenate(
                [z for b, at in enumerate(even) for z in (x[at], y[b * size : (b + 1) * size])], axis=0
            )
            for x, y in zip(state, part)
        ]
        level += 1
    for p in range(heads // 2):
        parts = [
            chunk_map(places[n], p, state[n * heads + 2 * p : n * heads + 2 * p + 2], keys_ref, values_ref, cols_ref)
            for n in range(chunks)
        ]
        while len(parts) > 1:
            parts = [composed(parts[n + 1], parts[n]) for n in range(0, len(parts), 2)]
        tiles[s * (heads // 2) + p] = parts[0]


def remote(src, dst, send, recv, to):
    return pltpu.make_async_remote_copy(
        src_ref=src, dst_ref=dst, send_sem=send, recv_sem=recv, device_id={"sp": to}, device_id_type=MESH
    )


def signal(semaphore, to):
    pl.semaphore_signal(semaphore, inc=1, device_id={"sp": to}, device_id_type=MESH)


def greet(ring, near, me, barrier):
    far = ring // near
    place, block = lax.rem(me, near), lax.div(me, near)
    for k in range(1, near):
        signal(barrier, block * near + lax.rem(place + k, near))

    @pl.when(block < far - 1)
    def _():
        for k in range(near):
            signal(barrier, (far - 1) * near + k)


def met(ring, near, me, barrier, ready):
    far = ring // near
    place, block = lax.rem(me, near), lax.div(me, near)
    pl.semaphore_wait(barrier, jnp.where(block == far - 1, ring - 1, near - 1))

    @pl.when((block == far - 1) & (place > 0))
    def _():
        signal(ready, 0)
        for b in range(far - 1):
            signal(ready, b * near + place)


def owner(pair):
    return jnp.maximum(pair, 1), jnp.where(pair == 0, 1, 0)


def exchange(ring, near, me, tiles, near_ref, sent_ref, far_ref, first_ref, rows_ref, final_ref, probe_ref, sems):
    recv1, send2, recv2, send_first, recv_first, send3, recv3, ready = sems
    far = ring // near
    place, block = lax.rem(me, near), lax.div(me, near)
    own = diagonal()
    i, j = iotas((LANES, LANES))

    firsts = []
    for pair in range(near):
        to, slot = max(pair, 1), int(pair == 0)
        firsts.append(
            remote(
                sent_ref.at[pair, :HEAD], first_ref.at[slot], send_first.at[pair], recv_first.at[slot],
                (far - 1) * near + to,
            )
        )

    @pl.when(me == 0)
    def _():
        for pair in range(near):
            tile = jnp.where(own, tiles[pair], 0.0)
            sent_ref[pair, :HEAD] = tile[:HEAD] + tile[HEAD:]
        pl.semaphore_wait(ready, near - 1)
        for copy in firsts:
            copy.start()

    outs = [
        remote(
            sent_ref.at[slot], far_ref.at[slot, jnp.minimum(block, far - 2)], send2.at[slot],
            recv2.at[slot, jnp.minimum(block, far - 2)], (far - 1) * near + place,
        )
        for slot in range(2)
    ]

    def final_copy(slot, pair, k):
        to = lax.rem(me + k, ring)
        return remote(rows_ref.at[slot, to], final_ref.at[pair], send3.at[slot, k], recv3.at[pair], to)

    @pl.when((block < far - 1) & (place > 0))
    def _():
        pl.semaphore_wait(ready, 1)

    for slot in (1, 0):
        pair = 0 if slot else place

        @pl.when((place == 1) if slot else (place > 0))
        def _():
            near_ref[slot, place] = tiles[pair]

            @pl.when(block == 0)
            def _():
                near_ref[slot, 0] = jnp.where(j == (i ^ HEAD), 1.0, 0.0)

            def arrived(k):
                @pl.when((place != k) & ((block > 0) | (k > 0)))
                def _():
                    remote(tiles.at[0], near_ref.at[slot, k], send2.at[0], recv1.at[slot, k], me).wait_recv()

            arrived(0)
            tile = near_ref[slot, 0]
            for k in range(1, near):
                arrived(k)
                tile = composed(near_ref[slot, k], tile)

            @pl.when(block < far - 1)
            def _():
                sent_ref[slot] = tile
                outs[slot].start()

            @pl.when(block == far - 1)
            def _():
                remote(sent_ref.at[0, :HEAD], first_ref.at[slot], send2.at[0], recv_first.at[slot], me).wait_recv()
                state = first_ref[slot]
                state = jnp.where(own, jnp.concatenate([state, state], axis=0), 0.0)
                for b in range(far - 1):
                    remote(sent_ref.at[0], far_ref.at[slot, b], send2.at[0], recv2.at[slot, b], me).wait_recv()
                    state = composed(far_ref[slot, b], state)
                state = jnp.where(own, composed(tile, state), 0.0)
                both = state[:HEAD] + state[HEAD:]
                rows = HEAD // ring
                read = matmul(jnp.broadcast_to(probe_ref[pl.ds(pair, 1), :], (8, LANES)), state)
                for d in range(ring):
                    rows_ref[slot, d, :rows] = both[d * rows : (d + 1) * rows]
                    rows_ref[slot, d, rows : rows + 1] = read[:1]

                @pl.loop(1, ring)
                def _(k):
                    final_copy(slot, pair, k).start()

                final_ref[pair] = rows_ref[slot, me]

    for pair in range(near):
        @pl.when((block < far - 1) | (place != max(pair, 1)))
        def _():
            remote(rows_ref.at[0, 0], final_ref.at[pair], send3.at[0, 0], recv3.at[pair], me).wait_recv()

    @pl.when(me == 0)
    def _():
        for copy in firsts:
            copy.wait_send()

    for slot in (1, 0):
        active = (place == 1) if slot else (place > 0)

        @pl.when(active & (block < far - 1))
        def _():
            outs[slot].wait_send()

        @pl.when(active & (block == far - 1))
        def _():
            @pl.loop(1, ring)
            def _(k):
                final_copy(slot, 0 if slot else place, k).wait_send()


def kernel(
    ring,
    heads,
    all_heads,
    x_hbm,
    wk_hbm,
    wv_hbm,
    wb_hbm,
    wf_hbm,
    speed_ref,
    extra_ref,
    probe_ref,
    states_ref,
    reads_ref,
    x_ref,
    w_ref,
    wg_ref,
    gate_ref,
    keys_ref,
    values_ref,
    cols_ref,
    turned_ref,
    low_ref,
    tiles,
    near_ref,
    sent_ref,
    far_ref,
    first_ref,
    rows_ref,
    final_ref,
    q_ref,
    gate_sems,
    w_sems,
    x_sems,
    send1,
    recv1,
    send2,
    recv2,
    send_first,
    recv_first,
    send3,
    recv3,
    ready,
):
    me = lax.axis_index("sp")
    width = heads * HEAD
    seqs, span, _ = x_hbm.shape
    pairs = heads // 2
    near = seqs * pairs
    far = ring // near
    barrier = pltpu.get_barrier_semaphore()
    gates = [
        pltpu.make_async_copy(wb_hbm, wg_ref.at[:all_heads], gate_sems.at[0]),
        pltpu.make_async_copy(wf_hbm, wg_ref.at[all_heads:], gate_sems.at[1]),
    ]
    for copy in gates:
        copy.start()
    depth = x_hbm.shape[2] // PIECES
    steps = span // ROWS
    first_pieces = []
    for k in range(PIECES):
        at = pl.ds(k * depth, depth)
        first_pieces.append([
            pltpu.make_async_copy(wk_hbm.at[at], w_ref.at[at, :width], w_sems.at[0, k]),
            pltpu.make_async_copy(wv_hbm.at[at], w_ref.at[at, width:], w_sems.at[1, k]),
            pltpu.make_async_copy(x_hbm.at[0, :ROWS, at], x_ref.at[:ROWS, at], w_sems.at[2, k]),
        ])
        for copy in first_pieces[-1]:
            copy.start()
    for step in range(1, seqs * steps):
        s, first = divmod(step * ROWS, span)
        pltpu.make_async_copy(
            x_hbm.at[s, pl.ds(first, ROWS)], x_ref.at[pl.ds(step * ROWS, ROWS)], x_sems.at[step]
        ).start()
    greet(ring, near, me, barrier)
    for s in range(seqs):
        for p in range(pairs):
            q_ref[s * pairs + p : s * pairs + p + 1, :] = probe_ref[s : s + 1, p * LANES : (p + 1) * LANES].astype(F32)

    for copy in gates:
        copy.wait()
    first = lax.axis_index("tp") * heads
    i, j = iotas((16, 2 * all_heads))
    taken = ((i < heads) & (j == first + i)) | ((i >= 8) & (i < 8 + heads) & (j == all_heads + first + i - 8))
    gate_ref[...] = dot(jnp.where(taken, 1.0, 0.0).astype(BF16), wg_ref[...]).astype(BF16)

    def taken_in(copies):
        def wait():
            for copy in copies:
                copy.wait()

        return wait

    refs = (x_ref, w_ref, gate_ref, extra_ref, speed_ref, keys_ref, values_ref, cols_ref, turned_ref)
    project(0, heads, [taken_in(copies) for copies in first_pieces], *refs)
    place, block = lax.rem(me, near), lax.div(me, near)

    def near_copy(pair):
        to, slot = owner(pair)
        return remote(
            tiles.at[pair], near_ref.at[slot, place], send1.at[pair], recv1.at[slot, place], block * near + to
        )

    @pl.loop(0, seqs)
    def _(s):
        @pl.loop(jnp.where(s == 0, 1, 0), steps)
        def _(part):
            step = s * steps + part
            arrival = pltpu.make_async_copy(
                x_hbm.at[0, pl.ds(0, ROWS)], x_ref.at[pl.ds(step * ROWS, ROWS)], x_sems.at[step]
            )
            project(step, heads, [arrival.wait], *refs)

        @pl.when(s == 0)
        def _():
            met(ring, near, me, barrier, ready)

        sequence_maps(
            s, span // CHUNK, heads, keys_ref, values_ref, cols_ref, turned_ref, low_ref, tiles
        )
        for p in range(pairs):
            pair = s * pairs + p

            @pl.when((me > 0) & (place != owner(pair)[0]))
            def _():
                near_copy(pair).start()

    exchange(
        ring, near, me, tiles, near_ref, sent_ref, far_ref, first_ref, rows_ref, final_ref, q_ref,
        (recv1, send2, recv2, send_first, recv_first, send3, recv3, ready),
    )
    for pair in range(near):
        @pl.when((me > 0) & (place != max(pair, 1)))
        def _():
            near_copy(pair).wait_send()

    rows = HEAD // ring
    _, lane = iotas((1, LANES))
    for s in range(seqs):
        for p in range(pairs):
            got = final_ref[s * pairs + p]
            states_ref[s, 2 * p] = got[:rows, :HEAD].astype(BF16)
            states_ref[s, 2 * p + 1] = swapped(got)[:rows, :HEAD].astype(BF16)
            read = got[rows : rows + 1]
            square = read * read
            even = jnp.sum(jnp.where(lane < HEAD, square, 0.0), axis=1, keepdims=True)
            odd = jnp.sum(jnp.where(lane < HEAD, 0.0, square), axis=1, keepdims=True)
            mean = jnp.where(lane < HEAD, even, odd) / HEAD
            reads_ref[s : s + 1, p * LANES : (p + 1) * LANES] = (read * lax.rsqrt(mean + 1e-06)).astype(BF16)


def body(
    ring,
    layer_feed,
    address_mapping,
    content_mapping,
    beta_mapping_matrix,
    forgetting_mapping,
    logged_fading_speed,
    extra_forgetting,
    opening_probe,
):
    seqs, span, depth = layer_feed.shape
    width = address_mapping.shape[1]
    heads = width // HEAD
    all_heads = beta_mapping_matrix.shape[1]
    tokens = seqs * span
    near = seqs * heads // 2
    places = tokens // CHUNK
    chains = span // CHUNK * heads
    hbm = pl.BlockSpec(memory_space=pl.ANY)
    vmem = pl.BlockSpec(memory_space=pltpu.VMEM)
    dma = pltpu.SemaphoreType.DMA
    return pl.pallas_call(
        functools.partial(kernel, ring, heads, all_heads),
        out_shape=(
            jax.ShapeDtypeStruct((seqs, heads, HEAD // ring, HEAD), BF16),
            jax.ShapeDtypeStruct((seqs, width), BF16),
        ),
        in_specs=[hbm] * 5 + [pl.BlockSpec(memory_space=pltpu.SMEM), vmem, vmem],
        out_specs=(vmem, vmem),
        scratch_shapes=[
            pltpu.VMEM((tokens, depth), BF16),
            pltpu.VMEM((depth, 2 * width), BF16),
            pltpu.VMEM((2 * all_heads, depth), BF16),
            pltpu.VMEM((16, depth), BF16),
            pltpu.VMEM((tokens, width), BF16),
            pltpu.VMEM((tokens, width), BF16),
            pltpu.VMEM((places, CHUNK, 16), F32),
            pltpu.VMEM((places, 16, LANES), F32),
            pltpu.VMEM((chains, CHUNK, CHUNK), BF16),
            pltpu.VMEM((near, LANES, LANES), F32),
            pltpu.VMEM((2, near, LANES, LANES), F32),
            pltpu.VMEM((near, LANES, LANES), F32),
            pltpu.VMEM((2, ring // near - 1, LANES, LANES), F32),
            pltpu.VMEM((2, HEAD, LANES), F32),
            pltpu.VMEM((2, ring, 8, LANES), F32),
            pltpu.VMEM((near, 8, LANES), F32),
            pltpu.VMEM((near, LANES), F32),
            dma((2,)),
            dma((3, PIECES)),
            dma((tokens // ROWS,)),
            dma((near,)),
            dma((2, near)),
            dma((2,)),
            dma((2, ring // near - 1)),
            dma((near,)),
            dma((2,)),
            dma((2, ring)),
            dma((near,)),
            pltpu.SemaphoreType.REGULAR,
        ],
        compiler_params=pltpu.CompilerParams(
            collective_id=0, has_side_effects=True, vmem_limit_bytes=56 * 1024 * 1024
        ),
    )(
        layer_feed,
        address_mapping,
        content_mapping,
        beta_mapping_matrix.T,
        forgetting_mapping.T,
        logged_fading_speed,
        extra_forgetting.transpose(0, 2, 1),
        opening_probe,
    )


def solution(mesh):
    in_specs = (
        P("grp", "sp", None),
        P(None, "tp"),
        P(None, "tp"),
        P(),
        P(),
        P("tp"),
        P("grp", "sp", "tp"),
        P("grp", "tp"),
    )
    out_specs = (P("grp", "tp", "sp", None), P("grp", "tp"))
    return jax.shard_map(
        functools.partial(body, mesh.shape["sp"]),
        mesh=mesh,
        in_specs=in_specs,
        out_specs=out_specs,
        check_vma=False,
    )
```

time: 74.8 us -> 64.5 us (0.86)
  the two profiles are of different devices: /device:TPU:160 before, /device:TPU:34 now
where the time goes in v3:
time: 64.5 us; the launch traced here: 64.3 us
  Pallas kernels  61.1 us (95%)
  local copies, waits for them, and re-layouts  2.52 us (4%)
    pallas_call x1, Pallas kernels, body(): pl.pallas_call(functools.partial(kernel, ring, heads, all_heads), out_sha...  61.1 us
    unnamed x2, local copies, waits for them, and re-layouts  2.52 us

profile of v3, /device:TPU:34, one launch (start us, length us, event | category | flops | bytes accessed | tf_op | source)
XLA Modules:
  0.0 64.3 jit_solution(6026541740259192179)
XLA Ops:
  0.6 61.1 %shard_map.95 = (bf16[2,4,4,64]{3,2,1,0:T(4,128)(2,1)}, bf16[2,256]{1,0:T(2,128)(2,1)}) custom-call(bf16[2,512,4096]{2,1,0:T(8,128)(2,1)} %x_hbm.1, bf16[4096,256]{1,0:T(8,128)(2,1)} %wk_hbm.1, bf16[4096,256]{1,0:T(8,128)(2,1)} %wv_hbm.1, bf16[32,4096]{1,0:T(8,128)(2,1)} %bitcast.3, bf16[32,4096]{1,0:T(8,128)(2,1)} %bitcast.4, f32[4]{0:T(128)} %speed_ref.1, ...), custom_call_target="tpu_custom_call" | custom-call | tf_op jit(solution)/shard_map/pallas_call | solution.py:534
  61.8 1.3 %copy.12 = bf16[2,4,4,64]{3,2,1,0:T(4,128)(2,1)} copy(bf16[2,4,4,64]{3,2,1,0:T(4,128)(2,1)} %get-tuple-element.4) | data formatting | bytes 8192
  63.1 1.2 %copy.13 = bf16[2,256]{1,0:T(2,128)(2,1)} copy(bf16[2,256]{1,0:T(2,128)(2,1)} %get-tuple-element.5) | data formatting | bytes 2048

commit v4 on v3

--- a/solution.py
+++ b/solution.py
@@ -12,6 +12,7 @@
 CHUNK = 128
 ROWS = 256
 PIECES = 4
+AHEAD = 3
 MESH = pl.DeviceIdType.MESH
 F32 = jnp.float32
 BF16 = jnp.bfloat16
@@ -61,27 +62,34 @@
     return x / (1.0 + jnp.exp(-x))
 
 
-def project(
-    step, heads, pieces, x_ref, w_ref, gate_ref, extra_ref, speed_ref, keys_ref, values_ref, cols_ref, turned_ref
-):
-    rows = pl.ds(pl.multiple_of(step * ROWS, ROWS), ROWS)
-    width = heads * HEAD
-    depth = x_ref.shape[1] // len(pieces)
+def project(step, pieces, x_ref, w_ref, gate_ref, raw_ref, pre_ref):
+    rows = pl.ds(step * ROWS, ROWS)
+    count = max(len(pieces), 1)
+    depth = x_ref.shape[1] // count
     both = pre = None
-    for k, arrive in enumerate(pieces):
-        arrive()
+    for k in range(count):
+        if pieces:
+            pieces[k]()
         at = slice(k * depth, (k + 1) * depth)
         x = x_ref[rows, at]
         part, gates = dot(x, w_ref[at, :]), dot(gate_ref[:, at], x, NT)
         both, pre = (part, gates) if k == 0 else (both + part, pre + gates)
-    both = both.astype(BF16).astype(F32)
-    pre = pre.astype(BF16).astype(F32)
-    keys = silu(both[:, :width])
+    raw_ref[rows, :] = both.astype(BF16)
+    pre_ref[step] = pre.astype(BF16).astype(F32)
+
+
+def chunk_parts(
+    step, heads, raw_ref, pre_ref, extra_ref, speed_ref, low_ref, inside_ref, start_ref, right_ref, carried_ref, closing_ref
+):
+    rows = pl.ds(step * ROWS, ROWS)
+    width = heads * HEAD
+    keys = silu(raw_ref[rows, :width].astype(F32))
     i, j = iotas((width, width))
     same = jnp.where(i // HEAD == j // HEAD, 1.0, 0.0).astype(BF16)
     squares = dot((keys * keys).astype(BF16), same)
-    keys_ref[rows, :] = (keys * lax.rsqrt(squares + 1e-06)).astype(BF16)
-    values_ref[rows, :] = silu(both[:, width:]).astype(BF16)
+    keys = keys * lax.rsqrt(squares + 1e-06)
+    values = silu(raw_ref[rows, width:].astype(F32))
+    pre = pre_ref[step]
 
     spans = extra_ref.shape[2] // ROWS
     at = pl.ds(pl.multiple_of(lax.rem(step, spans) * ROWS, ROWS), ROWS)
@@ -91,68 +99,62 @@
     speed = jnp.zeros((8, ROWS), F32)
     for h in range(heads):
         speed = jnp.where(i == h, speed_ref[h], speed)
-    beta = 1.0 / (1.0 + jnp.exp(-pre[:8]))
+    betas = 1.0 / (1.0 + jnp.exp(-pre[:8]))
     fade = pre[8:]
     plus = jnp.maximum(fade, 0.0) + jnp.log(1.0 + jnp.exp(-jnp.abs(fade)))
     decay = -jnp.exp(speed) * plus + extra
+
     i, j = iotas((CHUNK, CHUNK))
     until = jnp.where(i <= j, 1.0, 0.0)
+    left = j < HEAD
+    left_bf = jnp.where(left, 1.0, 0.0).astype(BF16)
+    near = jnp.where((i // SMALL) == (j // SMALL), 1.0, 0.0).astype(BF16)
+    r, l = iotas((SMALL, LANES))
+    c = l % SMALL
+    close = jnp.where(r > c, r ^ c, 0)
+    unit = jnp.where(r == c, 1.0, 0.0)
     for part in range(ROWS // CHUNK):
         at = slice(part * CHUNK, (part + 1) * CHUNK)
-        total = lax.dot_general(
+        totals = lax.dot_general(
             decay[:, at], until, NN, precision=lax.Precision.HIGHEST, preferred_element_type=F32
         )
-        mixed = jnp.concatenate([beta[:, at], total], axis=0)
-        place = step * (ROWS // CHUNK) + part
-        turned_ref[place] = mixed
-        cols_ref[place] = jnp.transpose(mixed)
-
-
-def lower_parts(place, p, keys_ref, cols_ref, turned_ref):
-    rows = pl.ds(pl.multiple_of(place * CHUNK, CHUNK), CHUNK)
-    i, j = iotas((CHUNK, CHUNK))
-    left = jnp.where(j < HEAD, 1.0, 0.0).astype(BF16)
-    keys = keys_ref[rows, p * LANES : (p + 1) * LANES]
-    even = keys * left
-    gram = dot(jnp.concatenate([even, keys - even], axis=0), keys, NT)
-    parts = []
-    for side in range(2):
-        h = 2 * p + side
-        beta = jnp.broadcast_to(cols_ref[place, :, h : h + 1], (CHUNK, LANES))
-        total = jnp.broadcast_to(cols_ref[place, :, 8 + h : 9 + h], (CHUNK, LANES))
-        ahead = jnp.broadcast_to(turned_ref[place, 8 + h : 9 + h, :], (CHUNK, LANES))
-        lower = beta * gram[side * CHUNK : (side + 1) * CHUNK] * jnp.exp(total - ahead)
-        parts.append(jnp.where(i > j, lower, 0.0).astype(BF16))
-    return parts
-
-
-def chunk_map(place, p, inverses, keys_ref, values_ref, cols_ref):
-    rows = pl.ds(pl.multiple_of(place * CHUNK, CHUNK), CHUNK)
-    pair = slice(p * LANES, (p + 1) * LANES)
-    i, j = iotas((CHUNK, CHUNK))
-    keys = keys_ref[rows, pair].astype(F32)
-    values = values_ref[rows, pair].astype(F32)
-    turned = swapped(keys)
-    carried, solved, closing = [], [], []
-    for h, inverse in zip((2 * p, 2 * p + 1), inverses):
-        mine = (j < HEAD) if h % 2 == 0 else (j >= HEAD)
-        beta = jnp.broadcast_to(cols_ref[place, :, h : h + 1], (CHUNK, LANES))
-        total = jnp.broadcast_to(cols_ref[place, :, 8 + h : 9 + h], (CHUNK, LANES))
-        right = beta * jnp.where(mine, values, -jnp.exp(total) * turned)
-        solved.append(dot(inverse, right.astype(BF16)).astype(BF16))
-        last = total[CHUNK - 1 :, :]
-        carried.append(jnp.where(mine, keys * jnp.exp(last - total), 0.0).astype(BF16))
-        closing.append(jnp.exp(last))
-    tile = dot(jnp.concatenate(carried, axis=0), jnp.concatenate(solved, axis=0), TN)
-    kept = jnp.where(i < HEAD, jnp.broadcast_to(closing[0], tile.shape), jnp.broadcast_to(closing[1], tile.shape))
-    return tile + jnp.where(j == (i ^ HEAD), kept, 0.0)
+        mixed = jnp.concatenate([betas[:, at], totals], axis=0)
+        cols = jnp.transpose(mixed)
+        for p in range(heads // 2):
+            pair = slice(p * LANES, (p + 1) * LANES)
+            k, v = keys[at, pair], values[at, pair]
+            turned = swapped(k)
+            kb = k.astype(BF16)
+            even = kb * left_bf
+            gram = dot(jnp.concatenate([even, kb - even], axis=0), kb, NT)
+            for side in range(2):
+                h = 2 * p + side
+                slot = (step * (ROWS // CHUNK) + part) * heads + h
+                mine = left if side == 0 else ~left
+                beta = jnp.broadcast_to(cols[:, h : h + 1], (CHUNK, LANES))
+                total = jnp.broadcast_to(cols[:, 8 + h : 9 + h], (CHUNK, LANES))
+                ahead = jnp.broadcast_to(mixed[8 + h : 9 + h, :], (CHUNK, LANES))
+                lower = beta * gram[side * CHUNK : (side + 1) * CHUNK] * jnp.exp(total - ahead)
+                lower = jnp.where(i > j, lower, 0.0).astype(BF16)
+                low_ref[slot] = lower
+                inside = lower * near
+                inside_ref[slot] = inside
+                packed = inside[:SMALL]
+                for b in range(1, CHUNK // SMALL):
+                    packed = packed + inside[b * SMALL : (b + 1) * SMALL]
+                start_ref[slot] = (unit - jnp.where(close == 1, packed.astype(F32), 0.0)).astype(BF16)
+                right_ref[slot] = (beta * jnp.where(mine, v, -jnp.exp(total) * turned)).astype(BF16)
+                last = total[CHUNK - 1 :, :]
+                carried_ref[slot] = jnp.where(mine, k * jnp.exp(last - total), 0.0).astype(BF16)
+                closing_ref[pl.ds(slot, 1), :] = jnp.exp(last)
 
 
 SMALL = 16
 
 
-def sequence_maps(s, chunks, heads, keys_ref, values_ref, cols_ref, turned_ref, low_ref, tiles):
-    places = [s * chunks + n for n in range(chunks)]
+def sequence_maps(s, chunks, heads, low_ref, inside_ref, start_ref, right_ref, carried_ref, closing_ref, tiles):
+    first = s * chunks * heads
+    slots = range(chunks * heads)
     count = CHUNK // SMALL
     i, j = iotas((CHUNK, CHUNK))
     same = jnp.where((i // SMALL) == (j // SMALL), 1.0, 0.0).astype(BF16)
@@ -160,22 +162,19 @@
     r, l = iotas((SMALL, LANES))
     c = l % SMALL
     close = jnp.where(r > c, r ^ c, 0)
-    unit = jnp.where(r == c, 1.0, 0.0)
-
-    state = []
-    for n in range(chunks):
-        for p in range(heads // 2):
-            for lower in lower_parts(places[n], p, keys_ref, cols_ref, turned_ref):
-                low_ref[len(state)] = lower
-                inside = lower * same
-                packed = inside[:SMALL]
-                for b in range(1, count):
-                    packed = packed + inside[b * SMALL : (b + 1) * SMALL]
-                state.append((unit - jnp.where(close == 1, packed.astype(F32), 0.0)).astype(BF16))
+
+    def by_two(lefts, rights):
+        out = []
+        for n in range(0, len(lefts), 2):
+            both = dot(jnp.concatenate(lefts[n : n + 2], axis=0), jnp.concatenate(rights[n : n + 2], axis=1))
+            out += [both[:SMALL, :LANES], both[SMALL:, LANES:]]
+        return out
+
+    state = [start_ref[first + slot] for slot in slots]
     level = 1
     while 2 << level <= SMALL:
-        inner = [dot(x, low_ref[slot] * same).astype(BF16) for slot, x in enumerate(state)]
-        inner = [dot(y, jnp.concatenate([x] * count, axis=0) * same) for x, y in zip(state, inner)]
+        inner = [y.astype(BF16) for y in by_two(state, [inside_ref[first + slot] for slot in slots])]
+        inner = by_two(inner, [jnp.concatenate([x] * count, axis=0) * same for x in state])
         state = [x - jnp.where((close >> level) == 1, y, 0.0).astype(BF16) for x, y in zip(state, inner)]
         level += 1
     state = [jnp.concatenate([x] * count, axis=0) * same for x in state]
@@ -185,7 +184,7 @@
         even = [slice(b * size, (b + 1) * size) for b in range(0, CHUNK // size, 2)]
         here = jnp.concatenate([apart[at] for at in odd], axis=0)
         part = [jnp.concatenate([x[at] for at in odd], axis=0) for x in state]
-        inner = [dot(x, low_ref[slot]).astype(BF16) for slot, x in enumerate(part)]
+        inner = [dot(x, low_ref[first + slot]).astype(BF16) for slot, x in enumerate(part)]
         inner = [dot(y, x) for y, x in zip(inner, state)]
         part = [x - jnp.where((here >> level) == 1, y, 0.0).astype(BF16) for x, y in zip(part, inner)]
         state = [
@@ -195,11 +194,17 @@
             for x, y in zip(state, part)
         ]
         level += 1
+    solved = [dot(x, right_ref[first + slot]).astype(BF16) for slot, x in enumerate(state)]
     for p in range(heads // 2):
-        parts = [
-            chunk_map(places[n], p, state[n * heads + 2 * p : n * heads + 2 * p + 2], keys_ref, values_ref, cols_ref)
-            for n in range(chunks)
-        ]
+        parts = []
+        for n in range(chunks):
+            slot = n * heads + 2 * p
+            carried = jnp.concatenate([carried_ref[first + slot], carried_ref[first + slot + 1]], axis=0)
+            tile = dot(carried, jnp.concatenate(solved[slot : slot + 2], axis=0), TN)
+            closing = [
+                jnp.broadcast_to(closing_ref[pl.ds(first + slot + side, 1), :], tile.shape) for side in range(2)
+            ]
+            parts.append(tile + jnp.where(j == (i ^ HEAD), jnp.where(i < HEAD, *closing), 0.0))
         while len(parts) > 1:
             parts = [composed(parts[n + 1], parts[n]) for n in range(0, len(parts), 2)]
         tiles[s * (heads // 2) + p] = parts[0]
@@ -376,11 +381,14 @@
     w_ref,
     wg_ref,
     gate_ref,
-    keys_ref,
-    values_ref,
-    cols_ref,
-    turned_ref,
+    raw_ref,
+    pre_ref,
     low_ref,
+    inside_ref,
+    start_ref,
+    right_ref,
+    carried_ref,
+    closing_ref,
     tiles,
     near_ref,
     sent_ref,
@@ -425,13 +433,18 @@
             pltpu.make_async_copy(wv_hbm.at[at], w_ref.at[at, width:], w_sems.at[1, k]),
             pltpu.make_async_copy(x_hbm.at[0, :ROWS, at], x_ref.at[:ROWS, at], w_sems.at[2, k]),
         ])
-        for copy in first_pieces[-1]:
-            copy.start()
+    later = []
     for step in range(1, seqs * steps):
         s, first = divmod(step * ROWS, span)
-        pltpu.make_async_copy(
-            x_hbm.at[s, pl.ds(first, ROWS)], x_ref.at[pl.ds(step * ROWS, ROWS)], x_sems.at[step]
-        ).start()
+        later.append([
+            pltpu.make_async_copy(
+                x_hbm.at[s, pl.ds(first, ROWS)], x_ref.at[pl.ds(step * ROWS, ROWS)], x_sems.at[step]
+            )
+        ])
+    queue = first_pieces + later
+    for copies in queue[:AHEAD]:
+        for copy in copies:
+            copy.start()
     greet(ring, near, me, barrier)
     for s in range(seqs):
         for p in range(pairs):
@@ -444,15 +457,30 @@
     taken = ((i < heads) & (j == first + i)) | ((i >= 8) & (i < 8 + heads) & (j == all_heads + first + i - 8))
     gate_ref[...] = dot(jnp.where(taken, 1.0, 0.0).astype(BF16), wg_ref[...]).astype(BF16)
 
-    def taken_in(copies):
+    def taken_in(k):
         def wait():
-            for copy in copies:
+            for copy in queue[k]:
                 copy.wait()
+            for copies in queue[k + AHEAD : k + AHEAD + 1] if k + 1 < PIECES else queue[k + AHEAD :]:
+                for copy in copies:
+                    copy.start()
 
         return wait
 
-    refs = (x_ref, w_ref, gate_ref, extra_ref, speed_ref, keys_ref, values_ref, cols_ref, turned_ref)
-    project(0, heads, [taken_in(copies) for copies in first_pieces], *refs)
+    project(0, [taken_in(k) for k in range(PIECES)], x_ref, w_ref, gate_ref, raw_ref, pre_ref)
+    parts = (low_ref, inside_ref, start_ref, right_ref, carried_ref, closing_ref)
+
+    @pl.loop(1, seqs * steps)
+    def _(step):
+        arrival = pltpu.make_async_copy(
+            x_hbm.at[0, pl.ds(0, ROWS)], x_ref.at[pl.ds(step * ROWS, ROWS)], x_sems.at[step]
+        )
+        arrival.wait()
+        chunk_parts(step - 1, heads, raw_ref, pre_ref, extra_ref, speed_ref, *parts)
+        project(step, [], x_ref, w_ref, gate_ref, raw_ref, pre_ref)
+
+    chunk_parts(seqs * steps - 1, heads, raw_ref, pre_ref, extra_ref, speed_ref, *parts)
+    met(ring, near, me, barrier, ready)
     place, block = lax.rem(me, near), lax.div(me, near)
 
     def near_copy(pair):
@@ -463,21 +491,7 @@
 
     @pl.loop(0, seqs)
     def _(s):
-        @pl.loop(jnp.where(s == 0, 1, 0), steps)
-        def _(part):
-            step = s * steps + part
-            arrival = pltpu.make_async_copy(
-                x_hbm.at[0, pl.ds(0, ROWS)], x_ref.at[pl.ds(step * ROWS, ROWS)], x_sems.at[step]
-            )
-            project(step, heads, [arrival.wait], *refs)
-
-        @pl.when(s == 0)
-        def _():
-            met(ring, near, me, barrier, ready)
-
-        sequence_maps(
-            s, span // CHUNK, heads, keys_ref, values_ref, cols_ref, turned_ref, low_ref, tiles
-        )
+        sequence_maps(s, span // CHUNK, heads, *parts, tiles)
         for p in range(pairs):
             pair = s * pairs + p
 
@@ -526,8 +540,7 @@
     all_heads = beta_mapping_matrix.shape[1]
     tokens = seqs * span
     near = seqs * heads // 2
-    places = tokens // CHUNK
-    chains = span // CHUNK * heads
+    chains = tokens // CHUNK * heads
     hbm = pl.BlockSpec(memory_space=pl.ANY)
     vmem = pl.BlockSpec(memory_space=pltpu.VMEM)
     dma = pltpu.SemaphoreType.DMA
@@ -544,11 +557,14 @@
             pltpu.VMEM((depth, 2 * width), BF16),
             pltpu.VMEM((2 * all_heads, depth), BF16),
             pltpu.VMEM((16, depth), BF16),
-            pltpu.VMEM((tokens, width), BF16),
-            pltpu.VMEM((tokens, width), BF16),
-            pltpu.VMEM((places, CHUNK, 16), F32),
-            pltpu.VMEM((places, 16, LANES), F32),
+            pltpu.VMEM((tokens, 2 * width), BF16),
+            pltpu.VMEM((tokens // ROWS, 16, ROWS), F32),
             pltpu.VMEM((chains, CHUNK, CHUNK), BF16),
+            pltpu.VMEM((chains, CHUNK, CHUNK), BF16),
+            pltpu.VMEM((chains, SMALL, CHUNK), BF16),
+            pltpu.VMEM((chains, CHUNK, CHUNK), BF16),
+            pltpu.VMEM((chains, CHUNK, CHUNK), BF16),
+            pltpu.VMEM((chains, LANES), F32),
             pltpu.VMEM((near, LANES, LANES), F32),
             pltpu.VMEM((2, near, LANES, LANES), F32),
             pltpu.VMEM((near, LANES, LANES), F32),

time: 64.5 us -> 62.6 us (0.971)
  Pallas kernels: 61.1 us -> 59.2 us
    pallas_call x1, Pallas kernels: 61.1 us -> 59.2 us  [body(): pl.pallas_call(functools.partial(kernel, ring, heads, all_heads), out_sha...]
where the time goes in v4:
time: 62.6 us; the launch traced here: 62.4 us
  Pallas kernels  59.2 us (95%)
  local copies, waits for them, and re-layouts  2.52 us (4%)
  between operations  0.64 us (1%)
    pallas_call x1, Pallas kernels, body(): pl.pallas_call(functools.partial(kernel, ring, heads, all_heads), out_sha...  59.2 us
    unnamed x2, local copies, waits for them, and re-layouts  2.52 us

profile of v4, /device:TPU:34, one launch (start us, length us, event | category | flops | bytes accessed | tf_op | source)
XLA Modules:
  0.0 62.4 jit_solution(608509143066093358)
XLA Ops:
  0.6 59.2 %shard_map.95 = (bf16[2,4,4,64]{3,2,1,0:T(4,128)(2,1)}, bf16[2,256]{1,0:T(2,128)(2,1)}) custom-call(bf16[2,512,4096]{2,1,0:T(8,128)(2,1)} %x_hbm.1, bf16[4096,256]{1,0:T(8,128)(2,1)} %wk_hbm.1, bf16[4096,256]{1,0:T(8,128)(2,1)} %wv_hbm.1, bf16[32,4096]{1,0:T(8,128)(2,1)} %bitcast.3, bf16[32,4096]{1,0:T(8,128)(2,1)} %bitcast.4, f32[4]{0:T(128)} %speed_ref.1, ...), custom_call_target="tpu_custom_call" | custom-call | tf_op jit(solution)/shard_map/pallas_call | solution.py:547
  59.8 1.3 %copy.12 = bf16[2,4,4,64]{3,2,1,0:T(4,128)(2,1)} copy(bf16[2,4,4,64]{3,2,1,0:T(4,128)(2,1)} %get-tuple-element.4) | data formatting | bytes 8192
  61.1 1.2 %copy.13 = bf16[2,256]{1,0:T(2,128)(2,1)} copy(bf16[2,256]{1,0:T(2,128)(2,1)} %get-tuple-element.5) | data formatting | bytes 2048

commit v5 on v4

--- a/solution.py
+++ b/solution.py
@@ -62,20 +62,22 @@
     return x / (1.0 + jnp.exp(-x))
 
 
-def project(step, pieces, x_ref, w_ref, gate_ref, raw_ref, pre_ref):
+def project(step, pieces, x_ref, w_ref, raw_ref):
     rows = pl.ds(step * ROWS, ROWS)
     count = max(len(pieces), 1)
     depth = x_ref.shape[1] // count
-    both = pre = None
+    both = None
     for k in range(count):
         if pieces:
             pieces[k]()
         at = slice(k * depth, (k + 1) * depth)
-        x = x_ref[rows, at]
-        part, gates = dot(x, w_ref[at, :]), dot(gate_ref[:, at], x, NT)
-        both, pre = (part, gates) if k == 0 else (both + part, pre + gates)
+        part = dot(x_ref[rows, at], w_ref[at, :])
+        both = part if k == 0 else both + part
     raw_ref[rows, :] = both.astype(BF16)
-    pre_ref[step] = pre.astype(BF16).astype(F32)
+
+
+def project_gates(step, x_ref, gate_ref, pre_ref):
+    pre_ref[step] = dot(gate_ref[...], x_ref[pl.ds(step * ROWS, ROWS), :], NT).astype(BF16).astype(F32)
 
 
 def chunk_parts(
@@ -152,13 +154,12 @@
 SMALL = 16
 
 
-def sequence_maps(s, chunks, heads, low_ref, inside_ref, start_ref, right_ref, carried_ref, closing_ref, tiles):
+def small_inverses(s, chunks, heads, inside_ref, start_ref):
     first = s * chunks * heads
     slots = range(chunks * heads)
     count = CHUNK // SMALL
     i, j = iotas((CHUNK, CHUNK))
     same = jnp.where((i // SMALL) == (j // SMALL), 1.0, 0.0).astype(BF16)
-    apart = jnp.where(i > j, i ^ j, 0)
     r, l = iotas((SMALL, LANES))
     c = l % SMALL
     close = jnp.where(r > c, r ^ c, 0)
@@ -177,7 +178,14 @@
         inner = by_two(inner, [jnp.concatenate([x] * count, axis=0) * same for x in state])
         state = [x - jnp.where((close >> level) == 1, y, 0.0).astype(BF16) for x, y in zip(state, inner)]
         level += 1
-    state = [jnp.concatenate([x] * count, axis=0) * same for x in state]
+    return [jnp.concatenate([x] * count, axis=0) * same for x in state]
+
+
+def sequence_maps(s, chunks, heads, state, low_ref, right_ref, carried_ref, closing_ref, tiles):
+    first = s * chunks * heads
+    i, j = iotas((CHUNK, CHUNK))
+    apart = jnp.where(i > j, i ^ j, 0)
+    level = SMALL.bit_length() - 1
     while 2 << level <= CHUNK:
         size = 1 << level
         odd = [slice(b * size, (b + 1) * size) for b in range(1, CHUNK // size, 2)]
@@ -244,10 +252,6 @@
             signal(ready, b * near + place)
 
 
-def owner(pair):
-    return jnp.maximum(pair, 1), jnp.where(pair == 0, 1, 0)
-
-
 def exchange(ring, near, me, tiles, near_ref, sent_ref, far_ref, first_ref, rows_ref, final_ref, probe_ref, sems):
     recv1, send2, recv2, send_first, recv_first, send3, recv3, ready = sems
     far = ring // near
@@ -372,11 +376,14 @@
     wv_hbm,
     wb_hbm,
     wf_hbm,
+    speed_hbm,
+    extra_hbm,
+    probe_hbm,
+    states_ref,
+    reads_ref,
     speed_ref,
     extra_ref,
     probe_ref,
-    states_ref,
-    reads_ref,
     x_ref,
     w_ref,
     wg_ref,
@@ -420,9 +427,10 @@
     gates = [
         pltpu.make_async_copy(wb_hbm, wg_ref.at[:all_heads], gate_sems.at[0]),
         pltpu.make_async_copy(wf_hbm, wg_ref.at[all_heads:], gate_sems.at[1]),
+        pltpu.make_async_copy(extra_hbm, extra_ref, gate_sems.at[2]),
+        pltpu.make_async_copy(probe_hbm, probe_ref, gate_sems.at[3]),
+        pltpu.make_async_copy(speed_hbm, speed_ref, gate_sems.at[4]),
     ]
-    for copy in gates:
-        copy.start()
     depth = x_hbm.shape[2] // PIECES
     steps = span // ROWS
     first_pieces = []
@@ -442,20 +450,13 @@
             )
         ])
     queue = first_pieces + later
-    for copies in queue[:AHEAD]:
+    for n, copies in enumerate(queue[:AHEAD]):
         for copy in copies:
             copy.start()
+        if n == 0:
+            for copy in gates:
+                copy.start()
     greet(ring, near, me, barrier)
-    for s in range(seqs):
-        for p in range(pairs):
-            q_ref[s * pairs + p : s * pairs + p + 1, :] = probe_ref[s : s + 1, p * LANES : (p + 1) * LANES].astype(F32)
-
-    for copy in gates:
-        copy.wait()
-    first = lax.axis_index("tp") * heads
-    i, j = iotas((16, 2 * all_heads))
-    taken = ((i < heads) & (j == first + i)) | ((i >= 8) & (i < 8 + heads) & (j == all_heads + first + i - 8))
-    gate_ref[...] = dot(jnp.where(taken, 1.0, 0.0).astype(BF16), wg_ref[...]).astype(BF16)
 
     def taken_in(k):
         def wait():
@@ -467,37 +468,58 @@
 
         return wait
 
-    project(0, [taken_in(k) for k in range(PIECES)], x_ref, w_ref, gate_ref, raw_ref, pre_ref)
+    project(0, [taken_in(k) for k in range(PIECES)], x_ref, w_ref, raw_ref)
+
+    for copy in gates:
+        copy.wait()
+    first = lax.axis_index("tp") * heads
+    i, j = iotas((16, 2 * all_heads))
+    taken = ((i < heads) & (j == first + i)) | ((i >= 8) & (i < 8 + heads) & (j == all_heads + first + i - 8))
+    gate_ref[...] = dot(jnp.where(taken, 1.0, 0.0).astype(BF16), wg_ref[...]).astype(BF16)
+    project_gates(0, x_ref, gate_ref, pre_ref)
+    for s in range(seqs):
+        for p in range(pairs):
+            q_ref[s * pairs + p : s * pairs + p + 1, :] = probe_ref[s : s + 1, p * LANES : (p + 1) * LANES].astype(F32)
     parts = (low_ref, inside_ref, start_ref, right_ref, carried_ref, closing_ref)
-
-    @pl.loop(1, seqs * steps)
+    total = seqs * steps
+
+    @pl.loop(1, total)
     def _(step):
         arrival = pltpu.make_async_copy(
             x_hbm.at[0, pl.ds(0, ROWS)], x_ref.at[pl.ds(step * ROWS, ROWS)], x_sems.at[step]
         )
         arrival.wait()
         chunk_parts(step - 1, heads, raw_ref, pre_ref, extra_ref, speed_ref, *parts)
-        project(step, [], x_ref, w_ref, gate_ref, raw_ref, pre_ref)
-
-    chunk_parts(seqs * steps - 1, heads, raw_ref, pre_ref, extra_ref, speed_ref, *parts)
+        project(step, [], x_ref, w_ref, raw_ref)
+        project_gates(step, x_ref, gate_ref, pre_ref)
+
     met(ring, near, me, barrier, ready)
     place, block = lax.rem(me, near), lax.div(me, near)
 
     def near_copy(pair):
-        to, slot = owner(pair)
+        to, slot = max(pair, 1), int(pair == 0)
         return remote(
             tiles.at[pair], near_ref.at[slot, place], send1.at[pair], recv1.at[slot, place], block * near + to
         )
 
-    @pl.loop(0, seqs)
-    def _(s):
-        sequence_maps(s, span // CHUNK, heads, *parts, tiles)
+    chunks = span // CHUNK
+    chunk_parts(total - 1, heads, raw_ref, pre_ref, extra_ref, speed_ref, *parts)
+    state = small_inverses(0, chunks, heads, inside_ref, start_ref)
+    for s in range(seqs):
+        if s + 1 < seqs:
+            following = small_inverses(s + 1, chunks, heads, inside_ref, start_ref)
+            for slot, x in enumerate(following):
+                inside_ref[(s + 1) * chunks * heads + slot] = x
+        sequence_maps(s, chunks, heads, state, low_ref, right_ref, carried_ref, closing_ref, tiles)
         for p in range(pairs):
             pair = s * pairs + p
 
-            @pl.when((me > 0) & (place != owner(pair)[0]))
+            @pl.when((me > 0) & (place != max(pair, 1)))
             def _():
                 near_copy(pair).start()
+
+        if s + 1 < seqs:
+            state = [inside_ref[(s + 1) * chunks * heads + slot] for slot in range(chunks * heads)]
 
     exchange(
         ring, near, me, tiles, near_ref, sent_ref, far_ref, first_ref, rows_ref, final_ref, q_ref,
@@ -550,9 +572,12 @@
             jax.ShapeDtypeStruct((seqs, heads, HEAD // ring, HEAD), BF16),
             jax.ShapeDtypeStruct((seqs, width), BF16),
         ),
-        in_specs=[hbm] * 5 + [pl.BlockSpec(memory_space=pltpu.SMEM), vmem, vmem],
+        in_specs=[hbm] * 8,
         out_specs=(vmem, vmem),
         scratch_shapes=[
+            pltpu.SMEM((heads,), F32),
+            pltpu.VMEM((seqs, heads, span), BF16),
+            pltpu.VMEM((seqs, width), BF16),
             pltpu.VMEM((tokens, depth), BF16),
             pltpu.VMEM((depth, 2 * width), BF16),
             pltpu.VMEM((2 * all_heads, depth), BF16),
@@ -573,7 +598,7 @@
             pltpu.VMEM((2, ring, 8, LANES), F32),
             pltpu.VMEM((near, 8, LANES), F32),
             pltpu.VMEM((near, LANES), F32),
-            dma((2,)),
+            dma((5,)),
             dma((3, PIECES)),
             dma((tokens // ROWS,)),
             dma((near,)),

time: 62.6 us -> 61.4 us (0.981)
  Pallas kernels: 59.2 us -> 58.1 us
    pallas_call x1, Pallas kernels: 59.2 us -> 58.1 us  [body(): pl.pallas_call(functools.partial(kernel, ring, heads, all_heads), out_sha...]
where the time goes in v5:
time: 61.4 us; the launch traced here: 61.3 us
  Pallas kernels  58.1 us (95%)
  local copies, waits for them, and re-layouts  2.52 us (4%)
  between operations  0.64 us (1%)
    pallas_call x1, Pallas kernels, body(): pl.pallas_call(functools.partial(kernel, ring, heads, all_heads), out_sha...  58.1 us
    unnamed x2, local copies, waits for them, and re-layouts  2.52 us

profile of v5, /device:TPU:34, one launch (start us, length us, event | category | flops | bytes accessed | tf_op | source)
XLA Modules:
  0.0 61.3 jit_solution(3134565968672969417)
XLA Ops:
  0.6 58.1 %shard_map.95 = (bf16[2,4,4,64]{3,2,1,0:T(4,128)(2,1)}, bf16[2,256]{1,0:T(2,128)(2,1)}) custom-call(bf16[2,512,4096]{2,1,0:T(8,128)(2,1)} %x_hbm.1, bf16[4096,256]{1,0:T(8,128)(2,1)} %wk_hbm.1, bf16[4096,256]{1,0:T(8,128)(2,1)} %wv_hbm.1, bf16[32,4096]{1,0:T(8,128)(2,1)} %bitcast.3, bf16[32,4096]{1,0:T(8,128)(2,1)} %bitcast.4, f32[4]{0:T(128)} %speed_hbm.1, ...), custom_call_target="tpu_custom_call" | custom-call | tf_op jit(solution)/shard_map/pallas_call | solution.py:569
  58.8 1.3 %copy.12 = bf16[2,4,4,64]{3,2,1,0:T(4,128)(2,1)} copy(bf16[2,4,4,64]{3,2,1,0:T(4,128)(2,1)} %get-tuple-element.4) | data formatting | bytes 8192
  60.1 1.2 %copy.13 = bf16[2,256]{1,0:T(2,128)(2,1)} copy(bf16[2,256]{1,0:T(2,128)(2,1)} %get-tuple-element.5) | data formatting | bytes 2048

commit v6 on v5

--- a/solution.py
+++ b/solution.py
@@ -232,7 +232,11 @@
     far = ring // near
     place, block = lax.rem(me, near), lax.div(me, near)
     for k in range(1, near):
-        signal(barrier, block * near + lax.rem(place + k, near))
+        to = block * near + lax.rem(place + k, near)
+
+        @pl.when((me > 0) & (to > 0))
+        def _():
+            signal(barrier, to)
 
     @pl.when(block < far - 1)
     def _():
@@ -243,7 +247,11 @@
 def met(ring, near, me, barrier, ready):
     far = ring // near
     place, block = lax.rem(me, near), lax.div(me, near)
-    pl.semaphore_wait(barrier, jnp.where(block == far - 1, ring - 1, near - 1))
+    count = jnp.where(block == far - 1, ring - 1, jnp.where(block == 0, near - 2, near - 1))
+
+    @pl.when(me > 0)
+    def _():
+        pl.semaphore_wait(barrier, count)
 
     @pl.when((block == far - 1) & (place > 0))
     def _():
@@ -469,6 +477,7 @@
         return wait
 
     project(0, [taken_in(k) for k in range(PIECES)], x_ref, w_ref, raw_ref)
+    met(ring, near, me, barrier, ready)
 
     for copy in gates:
         copy.wait()
@@ -493,7 +502,6 @@
         project(step, [], x_ref, w_ref, raw_ref)
         project_gates(step, x_ref, gate_ref, pre_ref)
 
-    met(ring, near, me, barrier, ready)
     place, block = lax.rem(me, near), lax.div(me, near)
 
     def near_copy(pair):

time: 61.4 us -> 60.8 us (level)
  no operation moved by 1% of the time
where the time goes in v6:
time: 60.8 us; the launch traced here: 60.7 us
  Pallas kernels  57.5 us (95%)
  local copies, waits for them, and re-layouts  2.52 us (4%)
  between operations  0.64 us (1%)
    pallas_call x1, Pallas kernels, body(): pl.pallas_call(functools.partial(kernel, ring, heads, all_heads), out_sha...  57.5 us
    unnamed x2, local copies, waits for them, and re-layouts  2.52 us

profile of v6, /device:TPU:34, one launch (start us, length us, event | category | flops | bytes accessed | tf_op | source)
XLA Modules:
  0.0 60.7 jit_solution(6142812291812686116)
XLA Ops:
  0.6 57.5 %shard_map.95 = (bf16[2,4,4,64]{3,2,1,0:T(4,128)(2,1)}, bf16[2,256]{1,0:T(2,128)(2,1)}) custom-call(bf16[2,512,4096]{2,1,0:T(8,128)(2,1)} %x_hbm.1, bf16[4096,256]{1,0:T(8,128)(2,1)} %wk_hbm.1, bf16[4096,256]{1,0:T(8,128)(2,1)} %wv_hbm.1, bf16[32,4096]{1,0:T(8,128)(2,1)} %bitcast.3, bf16[32,4096]{1,0:T(8,128)(2,1)} %bitcast.4, f32[4]{0:T(128)} %speed_hbm.1, ...), custom_call_target="tpu_custom_call" | custom-call | tf_op jit(solution)/shard_map/pallas_call | solution.py:577
  58.2 1.3 %copy.12 = bf16[2,4,4,64]{3,2,1,0:T(4,128)(2,1)} copy(bf16[2,4,4,64]{3,2,1,0:T(4,128)(2,1)} %get-tuple-element.4) | data formatting | bytes 8192
  59.5 1.2 %copy.13 = bf16[2,256]{1,0:T(2,128)(2,1)} copy(bf16[2,256]{1,0:T(2,128)(2,1)} %get-tuple-element.5) | data formatting | bytes 2048

commit v7 on v6

--- a/solution.py
+++ b/solution.py
@@ -387,8 +387,7 @@
     speed_hbm,
     extra_hbm,
     probe_hbm,
-    states_ref,
-    reads_ref,
+    final_ref,
     speed_ref,
     extra_ref,
     probe_ref,
@@ -410,7 +409,6 @@
     far_ref,
     first_ref,
     rows_ref,
-    final_ref,
     q_ref,
     gate_sems,
     w_sems,
@@ -538,6 +536,10 @@
         def _():
             near_copy(pair).wait_send()
 
+
+def finish(ring, final_ref, states_ref, reads_ref):
+    seqs, heads = states_ref.shape[:2]
+    pairs = heads // 2
     rows = HEAD // ring
     _, lane = iotas((1, LANES))
     for s in range(seqs):
@@ -574,14 +576,11 @@
     hbm = pl.BlockSpec(memory_space=pl.ANY)
     vmem = pl.BlockSpec(memory_space=pltpu.VMEM)
     dma = pltpu.SemaphoreType.DMA
-    return pl.pallas_call(
+    final = pl.pallas_call(
         functools.partial(kernel, ring, heads, all_heads),
-        out_shape=(
-            jax.ShapeDtypeStruct((seqs, heads, HEAD // ring, HEAD), BF16),
-            jax.ShapeDtypeStruct((seqs, width), BF16),
-        ),
+        out_shape=jax.ShapeDtypeStruct((near, 8, LANES), F32),
         in_specs=[hbm] * 8,
-        out_specs=(vmem, vmem),
+        out_specs=vmem,
         scratch_shapes=[
             pltpu.SMEM((heads,), F32),
             pltpu.VMEM((seqs, heads, span), BF16),
@@ -604,7 +603,6 @@
             pltpu.VMEM((2, ring // near - 1, LANES, LANES), F32),
             pltpu.VMEM((2, HEAD, LANES), F32),
             pltpu.VMEM((2, ring, 8, LANES), F32),
-            pltpu.VMEM((near, 8, LANES), F32),
             pltpu.VMEM((near, LANES), F32),
             dma((5,)),
             dma((3, PIECES)),
@@ -632,6 +630,15 @@
         extra_forgetting.transpose(0, 2, 1),
         opening_probe,
     )
+    return pl.pallas_call(
+        functools.partial(finish, ring),
+        out_shape=(
+            jax.ShapeDtypeStruct((seqs, heads, HEAD // ring, HEAD), BF16),
+            jax.ShapeDtypeStruct((seqs, width), BF16),
+        ),
+        in_specs=[vmem],
+        out_specs=(vmem, vmem),
+    )(final)
 
 
 def solution(mesh):

time: 60.8 us -> 59.6 us (0.980)
  local copies, waits for them, and re-layouts: 2.52 us -> 0 us
  Pallas kernels: 57.5 us -> 58.8 us
    unnamed x2 -> x0, local copies, waits for them, and re-layouts: 2.52 us -> none
    pallas_call x0 -> x1, Pallas kernels: none -> 1.41 us  [body(): pl.pallas_call(functools.partial(finish, ring), out_shape=(jax.ShapeDtype...]
where the time goes in v7:
time: 59.6 us; the launch traced here: 59.4 us
  Pallas kernels  58.8 us (99%)
  between operations  0.64 us (1%)
    pallas_call x1, Pallas kernels, body(): pl.pallas_call(functools.partial(kernel, ring, heads, all_heads), out_sha...  57.4 us
    pallas_call x1, Pallas kernels, body(): pl.pallas_call(functools.partial(finish, ring), out_shape=(jax.ShapeDtype...  1.41 us

profile of v7, /device:TPU:34, one launch (start us, length us, event | category | flops | bytes accessed | tf_op | source)
XLA Modules:
  0.0 59.4 jit_solution(2762154780348893870)
XLA Ops:
  0.6 57.4 %shard_map.95.final_ref = f32[4,8,128]{2,1,0:T(8,128)} custom-call(bf16[2,512,4096]{2,1,0:T(8,128)(2,1)} %x_hbm.1, bf16[4096,256]{1,0:T(8,128)(2,1)} %wk_hbm.1, bf16[4096,256]{1,0:T(8,128)(2,1)} %wv_hbm.1, bf16[32,4096]{1,0:T(8,128)(2,1)} %bitcast.3, bf16[32,4096]{1,0:T(8,128)(2,1)} %bitcast.4, f32[4]{0:T(128)} %speed_hbm.1, bf16[2,4,512]{2,1,0:T(4,128)(2,1)} %bitcast.5, ...), custom_call_target="tpu_custom_call" | custom-call | tf_op jit(solution)/shard_map/pallas_call | solution.py:579
  58.0 1.4 %shard_map.96 = (bf16[2,4,4,64]{3,2,1,0:T(4,128)(2,1)}, bf16[2,256]{1,0:T(2,128)(2,1)}) custom-call(f32[4,8,128]{2,1,0:T(8,128)} %shard_map.95.final_ref), custom_call_target="tpu_custom_call" | custom-call | tf_op jit(solution)/shard_map/pallas_call | solution.py:633
